TPU v7x, 128 devices: a whole 4x4x4 slice. The times are simulated.
128 devices in a mesh: ep: 128 (over z, y, x, core).
Axes of the slice: x: 4, y: 4, z: 4, core: 2. Of those that a mesh axis runs over, the one named last changes fastest.
Arguments:
- tokens: bfloat16 [512, 2048], P('ep'), may hold values from -6 to 6
- lengths: int32 [512], P('ep'), may hold values from 1 to 1023
- cache_keys: bfloat16 [512, 1024, 2, 128], P('ep')
- cache_values: bfloat16 [512, 1024, 2, 128], P('ep'), may hold values from -6 to 6
- query_w: bfloat16 [2048, 1024], replicated, may hold values from -0.125 to 0.125
- key_w: bfloat16 [2048, 256], replicated, may hold values from -0.125 to 0.125
- value_w: bfloat16 [2048, 256], replicated, may hold values from -0.125 to 0.125
- out_w: bfloat16 [1024, 2048], replicated, may hold values from -0.1875 to 0.1875
- mix_lambda: float32 [8], replicated, may hold values from 0.3 to 0.8
- head_gain: float32 [128], replicated, may hold values from 0.1 to 1.9
- attn_gain: float32 [2048], replicated, may hold values from 0.1 to 1.9
- ffn_gain: float32 [2048], replicated, may hold values from 0.1 to 1.9
- routes: int32 [512, 2], P('ep'), may hold values from 0 to 7, all different within a row; in each aligned block of 4 rows (0 to 3, 4 to 7, ...) at most 2 rows name the same one
- route_weights: float32 [512, 2], P('ep'), may hold values from 0.2 to 1
- exp_gate: bfloat16 [2048, 49152], P(None, 'ep'), may hold values from -0.125 to 0.125
- exp_up: bfloat16 [2048, 49152], P(None, 'ep'), may hold values from -0.125 to 0.125
- exp_down: bfloat16 [49152, 2048], P('ep'), may hold values from -0.078125 to 0.078125
- dense_gate: bfloat16 [128, 256, 352], P('ep'), may hold values from -0.125 to 0.125
- dense_up: bfloat16 [128, 256, 352], P('ep'), may hold values from -0.125 to 0.125
- dense_down: bfloat16 [128, 352, 256], P('ep'), may hold values from -0.078125 to 0.078125
- branch_gate: bfloat16 [2048], replicated, may hold values from -0.125 to 0.125
Outputs:
- output: bfloat16 [512, 2048], P('ep')
- new_keys: bfloat16 [512, 256], P('ep')
- new_values: bfloat16 [512, 256], P('ep')
Inputs may be any that keep to these rules, and one draw needn't show every extreme that they name: `routes`: each row names 2 different experts; among the 4 rows of one device no expert is named by more than 2 rows, a bound that some block reaches.
All inputs are finite; a program needn't handle non-finite values.
Results may differ from a plain program's by a relative error of at most 0.015.
Values may be sent and summed in bfloat16 or wider, within the bound.
A program may use at most 128 MiB of HBM per device.

v0:
```python
import jax
import jax.numpy as jnp
from jax import lax
from jax.sharding import PartitionSpec as P

HEADS = 8
KV_HEADS = 2
HEAD_DIM = 128
SEQ_DEV = 4
TOP_K = 2
SPLIT = 16


def sent_together(arrays, axis, split_dim, concat_dim, along):
    widths = [a.shape[along] for a in arrays]
    both = jnp.concatenate(arrays, axis=along)
    filled = lax.all_to_all(both, axis, split_axis=split_dim, concat_axis=concat_dim, tiled=True)
    return tuple(jnp.split(filled, [sum(widths[:k]) for k in range(1, len(widths))], axis=along))


def split_up(x, dim, peers):
    before, after = (x.shape[:dim], x.shape[dim + 1 :])
    return jnp.moveaxis(x.reshape(*before, peers, -1, *after), dim, 0)


def cut_rows(length, count):
    unit = 8 if length >= 8 * count else 1
    return [length // unit * k // count * unit for k in range(1, count)]


def in_order(tiles, dim):
    lengths = list(tiles.shape[1:])
    lengths[dim] *= tiles.shape[0]
    return jnp.moveaxis(tiles, 0, dim).reshape(lengths)


def exchange_in_pieces(x, axis, pieces, split_dim, concat_dim):
    tiles = split_up(x, split_dim, lax.axis_size(axis))
    cut = max(range(1, max(2, tiles.ndim - 1)), key=lambda d: tiles.shape[d])
    outs = []
    for piece in jnp.split(tiles, cut_rows(tiles.shape[cut], pieces), axis=cut):
        if piece.size:
            outs.append(lax.all_to_all(piece, axis, split_axis=0, concat_axis=0, tiled=True))
    return in_order(jnp.concatenate(outs, axis=cut), concat_dim)


def rms_norm(values, gain, epsilon):
    scale = lax.rsqrt(jnp.mean(values * values, axis=-1, keepdims=True) + epsilon)
    return values * scale * gain


def softmax_pair(scores, own_score, valid):
    masked = jnp.where(valid, scores, -jnp.inf)
    largest = jnp.maximum(jnp.max(masked, axis=-1), own_score)
    raised = jnp.where(valid, jnp.exp(scores - largest[..., None]), 0.0)
    own_raised = jnp.exp(own_score - largest)
    total = jnp.sum(raised, axis=-1) + own_raised
    return (raised / total[..., None], own_raised / total)


def swiglu_rows(chosen, w_gate, w_up, w_down):
    gate_part = jnp.dot(chosen, w_gate, preferred_element_type=jnp.float32)
    up_part = jnp.dot(chosen, w_up, preferred_element_type=jnp.float32)
    act = (jax.nn.silu(gate_part) * up_part).astype(jnp.bfloat16)
    return jnp.dot(act, w_down, preferred_element_type=jnp.float32)


def per_device(
    tokens,
    lengths,
    cache_keys,
    cache_values,
    query_w,
    key_w,
    value_w,
    out_w,
    mix_lambda,
    head_gain,
    attn_gain,
    ffn_gain,
    routes,
    route_weights,
    exp_gate,
    exp_up,
    exp_down,
    dense_gate,
    dense_up,
    dense_down,
    branch_gate,
):
    rows = tokens.shape[0]
    groups = HEADS // KV_HEADS
    half = HEAD_DIM // 2
    scale = (HEAD_DIM // 2) ** (-0.5)
    cache_len = cache_keys.shape[1]
    xfull = tokens.astype(jnp.float32)
    normed = rms_norm(xfull, attn_gain, 1e-06).astype(jnp.bfloat16)
    query = jnp.dot(normed, query_w, preferred_element_type=jnp.float32).astype(jnp.bfloat16)
    key_new = jnp.dot(normed, key_w, preferred_element_type=jnp.float32).astype(jnp.bfloat16)
    value_new = jnp.dot(normed, value_w, preferred_element_type=jnp.float32).astype(jnp.bfloat16)
    qheads = query.reshape(rows, KV_HEADS, groups, HEAD_DIM)
    knew = key_new.reshape(rows, KV_HEADS, HEAD_DIM)
    vnew = value_new.reshape(rows, KV_HEADS, HEAD_DIM)
    valid = (jnp.arange(cache_len, dtype=jnp.int32)[None, :] < lengths[:, None])[:, None, None, :]
    first = (
        jnp.einsum(
            "sgqd,spgd->sgqp",
            qheads[..., :half],
            cache_keys[..., :half],
            preferred_element_type=jnp.float32,
        )
        * scale
    )
    first_own = (
        jnp.einsum(
            "sgqd,sgd->sgq",
            qheads[..., :half],
            knew[..., :half],
            preferred_element_type=jnp.float32,
        )
        * scale
    )
    second = (
        jnp.einsum(
            "sgqd,spgd->sgqp",
            qheads[..., half:],
            cache_keys[..., half:],
            preferred_element_type=jnp.float32,
        )
        * scale
    )
    second_own = (
        jnp.einsum(
            "sgqd,sgd->sgq",
            qheads[..., half:],
            knew[..., half:],
            preferred_element_type=jnp.float32,
        )
        * scale
    )
    prob_one, own_one = softmax_pair(first, first_own, valid)
    prob_two, own_two = softmax_pair(second, second_own, valid)
    lam = mix_lambda.reshape(KV_HEADS, groups)
    weights = (prob_one - lam[None, :, :, None] * prob_two).astype(jnp.bfloat16)
    own_weights = (own_one - lam[None] * own_two).astype(jnp.bfloat16)
    mixed = jnp.einsum("sgqp,spgd->sgqd", weights, cache_values, preferred_element_type=jnp.float32)
    mixed = (
        mixed + own_weights.astype(jnp.float32)[..., None] * vnew.astype(jnp.float32)[:, :, None, :]
    )
    heads = rms_norm(mixed, head_gain, 1e-05).astype(jnp.bfloat16).reshape(rows, HEADS * HEAD_DIM)
    hidden_state = xfull + jnp.dot(heads, out_w, preferred_element_type=jnp.float32)
    ffn_in = rms_norm(hidden_state, ffn_gain, 1e-06).astype(jnp.bfloat16)
    devices = lax.axis_size("ep")
    experts = devices // SPLIT
    row_blocks = devices // SPLIT
    capacity = min(SEQ_DEV, max(2, SEQ_DEV * TOP_K * 2 // experts))
    slots = jnp.arange(capacity, dtype=jnp.int32)
    all_rows = lax.all_gather(ffn_in, "ep", axis=0, tiled=True)
    gate = jax.nn.sigmoid(jnp.dot(ffn_in, branch_gate, preferred_element_type=jnp.float32))
    position = lax.axis_index("ep")
    row_span = dense_gate.shape[1]
    col_span = dense_gate.shape[2]
    row_block = position // SPLIT
    columns = lax.dynamic_slice_in_dim(all_rows, row_block * row_span, row_span, 1)
    gate_tile = jnp.dot(columns, dense_gate[0], preferred_element_type=jnp.float32).reshape(
        devices, rows, col_span
    )
    up_tile = jnp.dot(columns, dense_up[0], preferred_element_type=jnp.float32).reshape(
        devices, rows, col_span
    )
    gate_in, up_in = tuple(
        (
            part.astype(jnp.float32)
            for part in sent_together(
                (gate_tile.astype(jnp.bfloat16), up_tile.astype(jnp.bfloat16)), "ep", 0, 0, 1
            )
        )
    )
    gate_sum = jnp.sum(gate_in.reshape(row_blocks, SPLIT, rows, col_span), axis=0)
    up_sum = jnp.sum(up_in.reshape(row_blocks, SPLIT, rows, col_span), axis=0)
    own_act = (jax.nn.silu(gate_sum) * up_sum).astype(jnp.bfloat16)
    outgoing_act = jnp.tile(own_act, (row_blocks, 1, 1))
    act_in = lax.all_to_all(outgoing_act, "ep", split_axis=0, concat_axis=0, tiled=True)
    down_tile = jnp.dot(
        act_in.reshape(devices * rows, col_span), dense_down[0], preferred_element_type=jnp.float32
    )
    down_in = lax.all_to_all(
        down_tile.reshape(devices, rows, row_span).astype(jnp.bfloat16),
        "ep",
        split_axis=0,
        concat_axis=0,
        tiled=True,
    ).astype(jnp.float32)
    down_sum = jnp.sum(down_in.reshape(row_blocks, SPLIT, rows, row_span), axis=1)
    dense = jnp.transpose(down_sum, (1, 0, 2)).reshape(rows, row_blocks * row_span)
    expert_ids = jnp.arange(experts, dtype=jnp.int32)
    match = routes[None, :, :] == expert_ids[:, None, None]
    weight = jnp.sum(jnp.where(match, route_weights[None], 0.0), axis=-1)
    hit = jnp.any(match, axis=-1).astype(jnp.int32)
    rank = jnp.cumsum(hit, axis=1) - 1
    select = (hit[:, None, :] == 1) & (rank[:, None, :] == slots[None, :, None])
    chosen = jnp.einsum(
        "ecs,sd->ecd", select.astype(jnp.bfloat16), ffn_in, preferred_element_type=jnp.float32
    ).astype(jnp.bfloat16)
    outgoing = jnp.repeat(chosen, SPLIT, axis=0)
    incoming = lax.all_to_all(outgoing, "ep", split_axis=0, concat_axis=0, tiled=True)
    sources = incoming.shape[0]
    taken = incoming.shape[1]
    result = swiglu_rows(incoming.reshape(sources * taken, -1), exp_gate, exp_up, exp_down)
    returned = exchange_in_pieces(
        result.reshape(sources, taken, -1).astype(jnp.bfloat16), "ep", 2, 0, 0
    ).astype(jnp.float32)
    summed = jnp.sum(returned.reshape(experts, SPLIT, capacity, -1), axis=1)
    weighted = select.astype(jnp.float32) * weight[:, None, :]
    routed = jnp.einsum("ecs,ecd->sd", weighted, summed, precision=lax.Precision.HIGHEST)
    output = (hidden_state + routed + gate[:, None] * dense).astype(jnp.bfloat16)
    return (output, key_new, value_new)


def solution(mesh):
    placed = (
        P("ep", None),
        P("ep"),
        P("ep", None, None, None),
        P("ep", None, None, None),
        P(),
        P(),
        P(),
        P(),
        P(),
        P(),
        P(),
        P(),
        P("ep", None),
        P("ep", None),
        P(None, "ep"),
        P(None, "ep"),
        P("ep", None),
        P("ep", None, None),
        P("ep", None, None),
        P("ep", None, None),
        P(),
    )
    return jax.shard_map(
        per_device,
        mesh=mesh,
        in_specs=placed,
        out_specs=(P("ep", None), P("ep", None), P("ep", None)),
        check_vma=False,
    )
```

profile of v0, /device:TPU:0, one launch (start us, length us, event | category | flops | bytes accessed | tf_op | source)
XLA Modules:
  0.0 198.4 jit_solution(3395068889452520648)
XLA Ops:
  8.2 2.9 %convolution_convert_fusion.5 = bf16[4,1024]{1,0:T(4,128)(2,1)S(1)} fusion(bf16[2048,1024]{1,0:T(8,128)(2,1)} %param.25, bf16[4,2048]{1,0:T(4,128)(2,1)} %param.21, f32[2048]{0:T(1024)} %param.31, f32[4]{0:T(128)S(1)} %add_rsqrt_fusion.2), kind=kOutput, calls=%fused_computation.22 | convolution fusion | flops 16814080 | bytes 4227088 | tf_op jit(solution)/shard_map/dot_general | solution.py:98
  11.3 6.8 %fusion.79 = (bf16[4,1024,2,64]{3,2,1,0:T(2,128)(2,1)}, bf16[4,1024,2,64]{3,2,1,0:T(2,128)(2,1)}) fusion(bf16[4,1024,2,128]{3,2,1,0:T(2,128)(2,1)} %param.23), kind=kLoop, calls=%fused_computation.114 | loop fusion | bytes 4194304 | tf_op jit(solution)/shard_map/slice | solution.py:127
  19.2 2.5 %select_reduce_fusion.1 = (f32[4,2,4]{2,1,0:T(2,128)S(1)}, f32[4,2,4,1024]{3,2,1,0:T(4,128)S(1)}) fusion(pred[4,1024]{1,0:T(4,128)(4,1)S(1)} %iota_compare_fusion, bf16[4,1024,2,64]{3,2,1,0:T(2,128)(2,1)} %get-tuple-element.6, bf16[4,2,4,128]{3,2,1,0:T(4,128)(2,1)S(1)} %reshape.159), kind=kOutput, calls=%fused_computation.52 | convolution fusion | flops 4292576 | bytes 1192064 | tf_op jit(solution)/shard_map/sgqd,spgd->sgqp/dot_general | solution.py:106
  23.5 3.0 %multiply_reduce_fusion = (f32[4]{0:T(128)S(1)}, f32[4,2048]{1,0:T(4,128)S(1)}) fusion(bf16[4,1024]{1,0:T(4,128)(2,1)S(1)} %reshape.161, bf16[1024,2048]{1,0:T(8,128)(2,1)} %param.28, bf16[4,2048]{1,0:T(4,128)(2,1)S(1)} %copy-done.6), kind=kOutput, calls=%fused_computation.70 | convolution fusion | flops 16809980 | bytes 4251664 | tf_op jit(solution)/shard_map/dot_general | solution.py:151
  27.7 1.6 broadcast_in_dim.69
  29.3 11.9 %all-to-all-start = ((bf16[128,2,2048]{2,1,0:T(2,128)(2,1)}), bf16[128,2,2048]{2,1,0:T(2,128)(2,1)}, u32[]{:S(2)}, u32[]{:S(2)}) async-start(bf16[128,2,2048]{2,1,0:T(2,128)(2,1)} %bitcast.7), calls=%async_computation | async-start | bytes 2097152 | tf_op jit(solution)/shard_map/all_to_all | solution.py:206
  41.3 18.7 %all-to-all-done = bf16[128,2,2048]{2,1,0:T(2,128)(2,1)} async-done(((bf16[128,2,2048]{2,1,0:T(2,128)(2,1)}), bf16[128,2,2048]{2,1,0:T(2,128)(2,1)}, u32[]{:S(2)}, u32[]{:S(2)}) %all-to-all-start) | async-done | bytes 1048608 | tf_op jit(solution)/shard_map/all_to_all | solution.py:206
  60.0 1.5 reshape.163
  61.4 2.9 %fusion.82 = f32[256,384]{1,0:T(8,128)} fusion(bf16[256,2048]{1,0:T(8,128)(2,1)S(1)} %reshape.163, bf16[2048,384]{1,0:T(8,128)(2,1)} %param.35), kind=kOutput, calls=%fused_computation.117 | convolution fusion | flops 402653184 | bytes 3014656 | tf_op jit(solution)/shard_map/dot_general | solution.py:62
  64.3 4.4 %convolution_convert_fusion = bf16[256,2048]{1,0:T(8,128)(2,1)} fusion(bf16[384,2048]{1,0:T(8,128)(2,1)} %param.37, bf16[256,2048]{1,0:T(8,128)(2,1)S(1)} %reshape.163, bf16[2048,384]{1,0:T(8,128)(2,1)} %param.36, f32[256,384]{1,0:T(8,128)} %fusion.82), kind=kOutput, calls=%fused_computation | convolution fusion | flops 806420480 | bytes 5636096 | tf_op jit(solution)/shard_map/dot_general | solution.py:65
  68.7 1.7 convert_element_type.121
  70.4 2.5 %fusion.80 = (bf16[128,1,1,2048]{3,2,1,0:T(2,128)(2,1)}, bf16[128,1,1,2048]{3,2,1,0:T(2,128)(2,1)}) fusion(bf16[128,1,2,2048]{3,2,1,0:T(2,128)(2,1)S(1)} %bitcast.73), kind=kLoop, calls=%fused_computation.115 | loop fusion | bytes 2097152 | tf_op jit(solution)/shard_map/split | solution.py:41
  73.4 4.7 %reduce = bf16[128,2048]{1,0:T(8,128)(2,1)S(1)} reduce(bf16[128,1,1,2048]{3,2,1,0:T(2,128)(2,1)} %get-tuple-element.8, bf16[]{:T(256)} %broadcast.142), dimensions={1,2}, to_apply=%get-tuple-element.8.reduce_sub_computation | reduce | bytes 1048578 | tf_op jit(solution)/shard_map/split | solution.py:41
  79.3 5.7 %all-to-all-start.2 = ((bf16[128,2,1024]{2,1,0:T(2,128)(2,1)}), bf16[128,2,1024]{2,1,0:T(2,128)(2,1)}, u32[]{:S(2)}, u32[]{:S(2)}) async-start(bf16[128,2,1024]{2,1,0:T(2,128)(2,1)} %reshape.192), calls=%async_computation.2 | async-start | bytes 1048576 | tf_op jit(solution)/shard_map/all_to_all | solution.py:43
  85.1 18.9 %all-gather.3.cloned.1.call-done = bf16[128,4,2048]{2,1,0:T(4,128)(2,1)} async-done(((bf16[1,4,2048]{2,1,0:T(4,128)(2,1)}), bf16[128,4,2048]{2,1,0:T(4,128)(2,1)}) %all-gather.3.cloned.1.call-update) | async-done | bytes 2097168 | tf_op jit(solution)/shard_map/all_gather | solution.py:158
  104.0 4.0 %reshape.180 = bf16[512,2048]{1,0:T(8,128)(2,1)} reshape(bf16[128,4,2048]{2,1,0:T(4,128)(2,1)} %all-gather.3.cloned.1.call-done) | data formatting | bytes 4194304
  110.5 2.4 %copy.84 = bf16[128,8,352]{2,1,0:T(8,128)(2,1)} copy(bf16[128,8,352]{0,2,1:T(8,128)(2,1)} %pad_maximum_fusion.1) | data formatting | bytes 1441792 | tf_op jit(solution)/shard_map/concatenate | solution.py:16
  113.0 7.1 %all-to-all-start.3 = ((bf16[128,8,352]{2,1,0:T(8,128)(2,1)}), bf16[128,8,352]{2,1,0:T(8,128)(2,1)}, u32[]{:S(2)}, u32[]{:S(2)}) async-start(bf16[128,8,352]{2,1,0:T(8,128)(2,1)} %copy.84), calls=%async_computation.3 | async-start | bytes 1572864 | tf_op jit(solution)/shard_map/all_to_all | solution.py:17
  120.1 4.4 %reduce.1 = bf16[128,2048]{1,0:T(8,128)(2,1)} reduce(bf16[128,1,1,2048]{3,2,1,0:T(2,128)(2,1)S(1)} %copy-done.1, bf16[]{:T(256)} %broadcast.142), dimensions={1,2}, to_apply=%get-tuple-element.7.reduce_sub_computation | reduce | bytes 1048578 | tf_op jit(solution)/shard_map/split | solution.py:41
  124.6 2.2 %reshape.194 = bf16[128,2,1024]{2,1,0:T(2,128)(2,1)} reshape(bf16[128,2048]{1,0:T(8,128)(2,1)} %reduce.1) | data formatting | bytes 1048576
  126.8 9.1 %all-to-all-done.3 = bf16[128,8,352]{2,1,0:T(8,128)(2,1)} async-done(((bf16[128,8,352]{2,1,0:T(8,128)(2,1)}), bf16[128,8,352]{2,1,0:T(8,128)(2,1)}, u32[]{:S(2)}, u32[]{:S(2)}) %all-to-all-start.3) | async-done | bytes 720928 | tf_op jit(solution)/shard_map/all_to_all | solution.py:17
  135.9 4.6 %all-to-all-start.1 = ((bf16[128,2,1024]{2,1,0:T(2,128)(2,1)}), bf16[128,2,1024]{2,1,0:T(2,128)(2,1)S(1)}, u32[]{:S(2)}, u32[]{:S(2)}) async-start(bf16[128,2,1024]{2,1,0:T(2,128)(2,1)} %reshape.194), calls=%async_computation.1 | async-start | bytes 1048576 | tf_op jit(solution)/shard_map/all_to_all | solution.py:43
  140.5 1.7 fusion.81
  143.6 10.4 %all-to-all-done.1 = bf16[128,2,1024]{2,1,0:T(2,128)(2,1)S(1)} async-done(((bf16[128,2,1024]{2,1,0:T(2,128)(2,1)}), bf16[128,2,1024]{2,1,0:T(2,128)(2,1)S(1)}, u32[]{:S(2)}, u32[]{:S(2)}) %all-to-all-start.1) | async-done | bytes 524320 | tf_op jit(solution)/shard_map/all_to_all | solution.py:43
  154.0 5.7 %all-to-all-start.4 = ((bf16[128,4,352]{2,1,0:T(4,128)(2,1)}), bf16[128,4,352]{2,1,0:T(4,128)(2,1)}, u32[]{:S(2)}, u32[]{:S(2)}) async-start(bf16[128,4,352]{2,1,0:T(4,128)(2,1)} %copy.87), calls=%async_computation.4 | async-start | bytes 786432 | tf_op jit(solution)/shard_map/all_to_all | solution.py:183
  159.9 3.6 %reshape.193 = bf16[128,1,1,2048]{3,2,1,0:T(2,128)(2,1)S(1)} reshape(bf16[128,2,1024]{2,1,0:T(2,128)(2,1)} %all-to-all-done.2) | data formatting | bytes 1048576
  163.5 4.4 %reshape.195 = bf16[128,1,1,2048]{3,2,1,0:T(2,128)(2,1)} reshape(bf16[128,2,1024]{2,1,0:T(2,128)(2,1)} %copy-done.2) | data formatting | bytes 1048576
  167.9 3.5 %all-to-all-done.4 = bf16[128,4,352]{2,1,0:T(4,128)(2,1)} async-done(((bf16[128,4,352]{2,1,0:T(4,128)(2,1)}), bf16[128,4,352]{2,1,0:T(4,128)(2,1)}, u32[]{:S(2)}, u32[]{:S(2)}) %all-to-all-start.4) | async-done | bytes 360480 | tf_op jit(solution)/shard_map/all_to_all | solution.py:183
  171.4 1.3 convolution_convert_fusion.4
  173.7 6.2 %all-to-all-start.5 = ((bf16[128,4,256]{2,1,0:T(4,128)(2,1)}), bf16[128,4,256]{2,1,0:T(4,128)(2,1)S(1)}, u32[]{:S(2)}, u32[]{:S(2)}) async-start(bf16[128,4,256]{2,1,0:T(4,128)(2,1)} %copy.89), calls=%async_computation.5 | async-start | bytes 524288 | tf_op jit(solution)/shard_map/all_to_all | solution.py:187
  179.8 3.5 %pad_maximum_fusion = bf16[128,1,2,2048]{3,2,1,0:T(2,128)(2,1)S(1)} fusion(bf16[128,1,1,2048]{3,2,1,0:T(2,128)(2,1)S(1)} %reshape.193, bf16[128,1,1,2048]{3,2,1,0:T(2,128)(2,1)} %reshape.195), kind=kLoop, calls=%fused_computation.30 | loop fusion | flops 2097152 | bytes 2097152 | tf_op jit(solution)/shard_map/concatenate | solution.py:44
  184.2 6.4 %all-to-all-done.5 = bf16[128,4,256]{2,1,0:T(4,128)(2,1)S(1)} async-done(((bf16[128,4,256]{2,1,0:T(4,128)(2,1)}), bf16[128,4,256]{2,1,0:T(4,128)(2,1)S(1)}, u32[]{:S(2)}, u32[]{:S(2)}) %all-to-all-start.5) | async-done | bytes 262176 | tf_op jit(solution)/shard_map/all_to_all | solution.py:187
  (91 shorter events, 13.9 us)
Async XLA Ops:
  7.2 15.6 %copy-start = (bf16[4,1024,2,128]{3,2,1,0:T(2,128)(2,1)S(1)}, bf16[4,1024,2,128]{3,2,1,0:T(2,128)(2,1)}, u32[]{:S(2)}) copy-start(bf16[4,1024,2,128]{3,2,1,0:T(2,128)(2,1)} %param.24) | copy-start | bytes 6291460
  7.2 96.8 %all-gather.3.cloned.1.call-start = ((), (), s32[]{:S(2)}) async-start(), calls=%async_computation.6 | async-start | bytes 2113536 | tf_op jit(solution)/shard_map/all_gather | solution.py:158
  8.2 2.9 %copy-start.17 = (s32[4]{0:T(128)S(1)}, s32[4]{0:T(128)}, u32[]{:S(2)}) copy-start(s32[4]{0:T(128)} %param.22) | copy-start | bytes 52
  11.3 6.8 %copy-start.4 = (bf16[2048,256]{1,0:T(8,128)(2,1)S(1)}, bf16[2048,256]{1,0:T(8,128)(2,1)}, u32[]{:S(2)}) copy-start(bf16[2048,256]{1,0:T(8,128)(2,1)} %param.26) | copy-start | bytes 3145732
  11.3 6.8 %copy-start.6 = (bf16[4,2048]{1,0:T(4,128)(2,1)S(1)}, bf16[4,2048]{1,0:T(4,128)(2,1)}, u32[]{:S(2)}) copy-start(bf16[4,2048]{1,0:T(4,128)(2,1)} %param.21) | copy-start | bytes 49156
  11.3 6.8 %copy-start.9 = (f32[2048]{0:T(1024)S(1)}, f32[2048]{0:T(1024)}, u32[]{:S(2)}) copy-start(f32[2048]{0:T(1024)} %param.31) | copy-start | bytes 24580
  11.3 7.5 %copy-start.18 = (f32[8]{0:T(128)S(1)}, f32[8]{0:T(128)}, u32[]{:S(2)}) copy-start(f32[8]{0:T(128)} %param.29) | copy-start | bytes 100
  11.3 7.6 %copy-start.5 = (bf16[2048,256]{1,0:T(8,128)(2,1)S(1)}, bf16[2048,256]{1,0:T(8,128)(2,1)}, u32[]{:S(2)}) copy-start(bf16[2048,256]{1,0:T(8,128)(2,1)} %param.27) | copy-start | bytes 3145732
  18.4 4.1 %copy-start.12 = (bf16[4,256]{1,0:T(4,128)(2,1)}, bf16[4,256]{1,0:T(4,128)(2,1)S(1)}, u32[]{:S(2)}) copy-start(bf16[4,256]{1,0:T(4,128)(2,1)S(1)} %convolution_convert_fusion.7) | copy-start | bytes 6148
  19.1 3.3 %copy-start.11 = (bf16[4,256]{1,0:T(4,128)(2,1)}, bf16[4,256]{1,0:T(4,128)(2,1)S(1)}, u32[]{:S(2)}) copy-start(bf16[4,256]{1,0:T(4,128)(2,1)S(1)} %convolution_convert_fusion.6) | copy-start | bytes 6148
  19.2 2.5 %copy-start.3 = (bf16[4,1024,2,64]{3,2,1,0:T(2,128)(2,1)S(1)}, bf16[4,1024,2,64]{3,2,1,0:T(2,128)(2,1)}, u32[]{:S(2)}) copy-start(bf16[4,1024,2,64]{3,2,1,0:T(2,128)(2,1)} %get-tuple-element.5) | copy-start | bytes 3145732
  22.7 0.7 copy-start.16
  23.5 3.0 %copy-start.10 = (f32[2048]{0:T(1024)S(1)}, f32[2048]{0:T(1024)}, u32[]{:S(2)}) copy-start(f32[2048]{0:T(1024)} %param.32) | copy-start | bytes 24580
  23.5 3.7 %copy-start.14 = (s32[4,2]{0,1:T(2,128)S(1)}, s32[4,2]{0,1:T(2,128)}, u32[]{:S(2)}) copy-start(s32[4,2]{0,1:T(2,128)} %param.33) | copy-start | bytes 100
  29.3 30.6 %all-to-all-start = ((bf16[128,2,2048]{2,1,0:T(2,128)(2,1)}), bf16[128,2,2048]{2,1,0:T(2,128)(2,1)}, u32[]{:S(2)}, u32[]{:S(2)}) async-start(bf16[128,2,2048]{2,1,0:T(2,128)(2,1)} %bitcast.7), calls=%async_computation | async-start | bytes 2097152 | tf_op jit(solution)/shard_map/all_to_all | solution.py:206
  79.3 33.6 %all-to-all-start.2 = ((bf16[128,2,1024]{2,1,0:T(2,128)(2,1)}), bf16[128,2,1024]{2,1,0:T(2,128)(2,1)}, u32[]{:S(2)}, u32[]{:S(2)}) async-start(bf16[128,2,1024]{2,1,0:T(2,128)(2,1)} %reshape.192), calls=%async_computation.2 | async-start | bytes 1048576 | tf_op jit(solution)/shard_map/all_to_all | solution.py:43
  85.1 23.9 %copy-start.7 = (bf16[1,256,352]{1,2,0:T(8,128)(2,1)S(1)}, bf16[1,256,352]{1,2,0:T(8,128)(2,1)}, u32[]{:S(2)}) copy-start(bf16[1,256,352]{1,2,0:T(8,128)(2,1)} %param.39) | copy-start | bytes 540676
  85.1 24.2 %copy-start.8 = (bf16[1,256,352]{1,2,0:T(8,128)(2,1)S(1)}, bf16[1,256,352]{1,2,0:T(8,128)(2,1)}, u32[]{:S(2)}) copy-start(bf16[1,256,352]{1,2,0:T(8,128)(2,1)} %param.38) | copy-start | bytes 540676
  109.6 10.5 %copy-start.1 = (bf16[128,1,1,2048]{3,2,1,0:T(2,128)(2,1)S(1)}, bf16[128,1,1,2048]{3,2,1,0:T(2,128)(2,1)}, u32[]{:S(2)}) copy-start(bf16[128,1,1,2048]{3,2,1,0:T(2,128)(2,1)} %get-tuple-element.7) | copy-start | bytes 1572868
  113.0 22.9 %all-to-all-start.3 = ((bf16[128,8,352]{2,1,0:T(8,128)(2,1)}), bf16[128,8,352]{2,1,0:T(8,128)(2,1)}, u32[]{:S(2)}, u32[]{:S(2)}) async-start(bf16[128,8,352]{2,1,0:T(8,128)(2,1)} %copy.84), calls=%async_computation.3 | async-start | bytes 1572864 | tf_op jit(solution)/shard_map/all_to_all | solution.py:17
  135.9 18.1 %all-to-all-start.1 = ((bf16[128,2,1024]{2,1,0:T(2,128)(2,1)}), bf16[128,2,1024]{2,1,0:T(2,128)(2,1)S(1)}, u32[]{:S(2)}, u32[]{:S(2)}) async-start(bf16[128,2,1024]{2,1,0:T(2,128)(2,1)} %reshape.194), calls=%async_computation.1 | async-start | bytes 1048576 | tf_op jit(solution)/shard_map/all_to_all | solution.py:43
  142.2 17.4 %copy-start.13 = (bf16[2048]{0:T(1024)(128)(2,1)S(1)}, bf16[2048]{0:T(1024)(128)(2,1)}, u32[]{:S(2)}) copy-start(bf16[2048]{0:T(1024)(128)(2,1)} %param.41) | copy-start | bytes 12292
  142.3 17.4 %copy-start.15 = (f32[4,2]{0,1:T(2,128)S(1)}, f32[4,2]{0,1:T(2,128)}, u32[]{:S(2)}) copy-start(f32[4,2]{0,1:T(2,128)} %param.34) | copy-start | bytes 100
  154.0 5.8 %copy-start.2 = (bf16[128,2,1024]{2,1,0:T(2,128)(2,1)}, bf16[128,2,1024]{2,1,0:T(2,128)(2,1)S(1)}, u32[]{:S(2)}) copy-start(bf16[128,2,1024]{2,1,0:T(2,128)(2,1)S(1)} %all-to-all-done.1) | copy-start | bytes 1572868
  154.0 17.4 %all-to-all-start.4 = ((bf16[128,4,352]{2,1,0:T(4,128)(2,1)}), bf16[128,4,352]{2,1,0:T(4,128)(2,1)}, u32[]{:S(2)}, u32[]{:S(2)}) async-start(bf16[128,4,352]{2,1,0:T(4,128)(2,1)} %copy.87), calls=%async_computation.4 | async-start | bytes 786432 | tf_op jit(solution)/shard_map/all_to_all | solution.py:183
  173.7 16.9 %all-to-all-start.5 = ((bf16[128,4,256]{2,1,0:T(4,128)(2,1)}), bf16[128,4,256]{2,1,0:T(4,128)(2,1)S(1)}, u32[]{:S(2)}, u32[]{:S(2)}) async-start(bf16[128,4,256]{2,1,0:T(4,128)(2,1)} %copy.89), calls=%async_computation.5 | async-start | bytes 524288 | tf_op jit(solution)/shard_map/all_to_all | solution.py:187
Sparse Core Ops, SparseCore 0:
  27.3 76.5 all-gather.2
where the time goes:
time: 200 us; the launch traced here: 198 us
  waiting for transfers between devices  66.9 us (33%)
  starting transfers between devices  41.2 us (21%)
  local copies, waits for them, and re-layouts  37.7 us (19%)
  matrix products  21 us (10%)
  other arithmetic  17.1 us (9%)
  between operations  14.5 us (7%)
    all_gather x1, waiting for transfers between devices, per_device(): all_rows = lax.all_gather(ffn_in, 'ep', axis=0, tiled=True)  18.9 us
    all_to_all x1, waiting for transfers between devices, per_device(): lax.all_to_all(outgoing, 'ep', split_axis=0, concat_axis=0, tiled=True)  18.7 us
    unnamed x46, local copies, waits for them, and re-layouts  15.6 us
    all_to_all x1, starting transfers between devices, per_device(): lax.all_to_all(outgoing, 'ep', split_axis=0, concat_axis=0, tiled=True)  11.9 us
    all_to_all x2, waiting for transfers between devices, exchange_in_pieces(): lax.all_to_all(piece, axis, split_axis=0, concat_axis=0, tiled=True)  10.4 us
    all_to_all x2, starting transfers between devices, exchange_in_pieces(): lax.all_to_all(piece, axis, split_axis=0, concat_axis=0, tiled=True)  10.3 us
    split x2, other arithmetic, exchange_in_pieces(): jnp.split(tiles, cut_rows(tiles.shape[cut], pieces), axis=cut)  9.14 us
    all_to_all x1, waiting for transfers between devices, sent_together(): lax.all_to_all(both, axis, split_axis=split_dim, concat_axis=concat_dim,...  9.06 us
  transfers between devices with their start and end apart: 7, of which 6 were waited for; matrix products, arithmetic and copies ran while one was open for 27% of the time, Pallas kernels for 0%

commit v1 on v0

v1 whole, which is shorter than its diff:
```python
import functools

import jax
import jax.numpy as jnp
from jax import lax
from jax.experimental import pallas as pl
from jax.experimental.pallas import tpu as pltpu
from jax.sharding import PartitionSpec as P

HEADS = 8
KV_HEADS = 2
HEAD_DIM = 128
SEQ_DEV = 4
SPLIT = 16
EXPERTS = 8
D = 2048
SIDE = 128
WIDE = D + SIDE
HID = 384
PART = 48
CHUNKS = 4
COLS = D // CHUNKS
MESH = pl.DeviceIdType.MESH
NT = (((1,), (1,)), ((), ()))


def rms_norm(values, gain, epsilon):
    scale = lax.rsqrt(jnp.mean(values * values, axis=-1, keepdims=True) + epsilon)
    return values * scale * gain


def softmax_pair(scores, own_score, valid):
    masked = jnp.where(valid, scores, -jnp.inf)
    largest = jnp.maximum(jnp.max(masked, axis=-1), own_score)
    raised = jnp.where(valid, jnp.exp(scores - largest[..., None]), 0.0)
    own_raised = jnp.exp(own_score - largest)
    total = jnp.sum(raised, axis=-1) + own_raised
    return (raised / total[..., None], own_raised / total)


def remote(src, dst, send, recv, device):
    return pltpu.make_async_remote_copy(
        src_ref=src, dst_ref=dst, send_sem=send, recv_sem=recv,
        device_id=(device,), device_id_type=MESH,
    )


def rows16(block, count=16):
    return pl.ds(pl.multiple_of(block * 16, 16), count)


def ffn_kernel(
    x_ref, hid_ref, wg_hbm, wu_hbm, wd_hbm, dg_ref, du_ref, dd_ref,
    out_ref,
    wgu, wdx, wsend, wrecv, own4, pack, xown, xpart, act, acc, psend, drecv, csend, crecv,
    bsum, bsend, brecv, fa, aown, asend, arecv,
    wsem, rs_w, rr_w, as_s, as_r, bs_s, bs_r, cs_s, cs_r, ds_s, ds_r,
    d2s, d2r, c2s, c2r, b2s, b2r, a2s, a2r,
):
    me = lax.axis_index("ep")
    core = lax.rem(me, 2)
    x = lax.rem(lax.div(me, 2), 4)
    y = lax.rem(lax.div(me, 8), 4)
    z = lax.div(me, 32)
    other = 1 - core
    a, sa = x * other + y * core, 2 * other + 8 * core
    b, sb = y * other + z * core, 8 * other + 32 * core
    c, sc = z * other + x * core, 32 * other + 2 * core
    row_block = lax.div(me, SPLIT)
    partner = me + other - core

    def ring(coord, stride, d):
        new = lax.rem(coord + d, 4)
        return new, me + (new - coord) * stride

    def group(d):
        new = lax.rem(row_block + d, 8)
        return new, me + (new - row_block) * SPLIT

    loads = []
    for n in range(3):
        cols = pl.ds(128 * n, 128)
        loads.append(pltpu.make_async_copy(wg_hbm.at[:, cols], wgu.at[n, :, pl.ds(0, 128)], wsem.at[2 * n]))
        loads.append(pltpu.make_async_copy(wu_hbm.at[:, cols], wgu.at[n, :, pl.ds(128, 128)], wsem.at[2 * n + 1]))
    loads.append(pltpu.make_async_copy(wd_hbm, wdx.at[pl.ds(0, HID)], wsem.at[6]))
    for load in loads:
        load.start()

    barrier = pltpu.get_barrier_semaphore()
    for coord, stride in ((a, sa), (b, sb), (c, sc)):
        for d in (1, 2, 3):
            pl.semaphore_signal(barrier, inc=1, device_id=(ring(coord, stride, d)[1],), device_id_type=MESH)
    for d in range(1, 8):
        pl.semaphore_signal(barrier, inc=1, device_id=(group(d)[1],), device_id_type=MESH)
    pl.semaphore_signal(barrier, inc=1, device_id=(partner,), device_id_type=MESH)
    pl.semaphore_wait(barrier, 17)

    sends = []

    def start(*args):
        copy = remote(*args)
        copy.start()
        sends.append(copy)
        return copy

    arrive_a = [start(x_ref, own4.at[a], as_s.at[d], as_r.at[d], ring(a, sa, d + 1)[1]) for d in range(3)]
    own4[a] = x_ref[...]

    eye = (
        lax.broadcasted_iota(jnp.int32, (384, 352), 0) == lax.broadcasted_iota(jnp.int32, (384, 352), 1)
    ).astype(jnp.bfloat16)
    gate_t = lax.dot_general(eye, dg_ref[...], NT, preferred_element_type=jnp.float32).astype(jnp.bfloat16)
    up_t = lax.dot_general(eye, du_ref[...], NT, preferred_element_type=jnp.float32).astype(jnp.bfloat16)
    for r in range(8):
        wsend[r, 0:PART] = gate_t[PART * r : PART * (r + 1)]
        wsend[r, PART : 2 * PART] = up_t[PART * r : PART * (r + 1)]
        if r < 7:
            wsend[r, 2 * PART :] = dd_ref[PART * r : PART * (r + 1)]
        else:
            wsend[r, 2 * PART : 2 * PART + 16] = dd_ref[336:352]
            wsend[r, 2 * PART + 16 :] = jnp.zeros((32, 256), jnp.bfloat16)
    arrive_w = []
    for d in range(7):
        to, device = group(d + 1)
        arrive_w.append(start(wsend.at[to], wrecv.at[row_block], rs_w.at[d], rr_w.at[d], device))
    wrecv[row_block] = wsend[row_block]

    for copy in arrive_a:
        copy.wait_recv()
    for j in range(4):
        pack[4 * j : 4 * j + 4] = own4[j].astype(jnp.float32)
    mine = 4 * c + b
    xown[rows16(mine)] = pack[...].astype(jnp.bfloat16)

    arrive_b = [
        start(xown.at[rows16(mine)], xown.at[rows16(mine)], bs_s.at[d], bs_r.at[d], ring(b, sb, d + 1)[1])
        for d in range(3)
    ]
    arrive_c, arrive_d = {}, []

    def spread(db):
        block = 4 * c + lax.rem(b + 4 - db, 4)
        for dc in (1, 3, 2):
            arrive_c[db, dc] = start(
                xown.at[rows16(block)], xown.at[rows16(block)],
                cs_s.at[3 * db + dc - 1], cs_r.at[3 * db + dc - 1], ring(c, sc, dc)[1],
            )
        across(block)

    def across(block):
        k = len(arrive_d)
        arrive_d.append(start(xown.at[rows16(block)], xpart.at[rows16(block)], ds_s.at[k], ds_r.at[k], partner))

    spread(0)
    for db in (1, 3, 2):
        arrive_b[db - 1].wait_recv()
        spread(db)
    for db in (0, 1, 3, 2):
        for dc in (1, 3, 2):
            arrive_c[db, dc].wait_recv()
            across(4 * lax.rem(c + 4 - dc, 4) + lax.rem(b + 4 - db, 4))

    for load in loads:
        load.wait()
    for copy in arrive_w:
        copy.wait_recv()
    wdx[HID + PART :] = jnp.zeros((128 - PART, D), jnp.bfloat16)
    for r in range(8):
        wdx[HID : HID + PART, 256 * r : 256 * (r + 1)] = wrecv[r, 2 * PART :]

    lane = lax.broadcasted_iota(jnp.int32, (256, SIDE), 1)

    def hidden(rows, k):
        side = rows[:, D:].astype(jnp.float32)
        expert = lax.div(me, SPLIT)
        weight = jnp.sum(jnp.where((lane == expert) | (lane == expert + 8), side, 0.0), axis=1, keepdims=True)
        gate = jnp.sum(jnp.where((lane == 16) | (lane == 17), side, 0.0), axis=1, keepdims=True)
        for n in range(3):
            both = jnp.dot(rows[:, :D], wgu[n], preferred_element_type=jnp.float32)
            first, second = both[:, :128], both[:, 128:]
            act[k, :, 128 * n : 128 * (n + 1)] = (first * jax.nn.sigmoid(first) * second * weight).astype(jnp.bfloat16)
        both = jnp.zeros((256, 128), jnp.float32)
        for r in range(8):
            both += lax.dot_general(
                rows[:, 256 * r : 256 * (r + 1)], wrecv[r, 0:128], NT, preferred_element_type=jnp.float32
            )
        second = pltpu.roll(both, 128 - PART, 1)
        value = both * jax.nn.sigmoid(both) * second * gate
        act[k, :, HID:] = jnp.where(lane < PART, value, 0.0).astype(jnp.bfloat16)

    hidden(xown, 0)
    for copy in arrive_d:
        copy.wait_recv()
    hidden(xpart, 1)

    arrive_2 = []
    for n in range(CHUNKS):
        cols = slice(COLS * n, COLS * (n + 1))
        psend[n] = jnp.dot(act[1], wdx[:, cols], preferred_element_type=jnp.float32).astype(jnp.bfloat16)
        arrive_2.append(start(psend.at[n], drecv.at[n], d2s.at[n], d2r.at[n], partner))
        acc[n] = jnp.dot(act[0], wdx[:, cols], preferred_element_type=jnp.float32)

    def ahead(n, coord, stride, src, dst, send_sem, recv_sem, height):
        copies = []
        for d in (1, 3, 2):
            to, device = ring(coord, stride, d)
            k = 3 * n + d - 1
            copies.append(
                start(
                    src.at[n, pl.ds(pl.multiple_of(to * height, height), height)], dst.at[n, d - 1],
                    send_sem.at[k], recv_sem.at[k], device,
                )
            )
        return copies

    arrive_c2 = []
    for n in range(CHUNKS):
        arrive_2[n].wait_recv()
        total = acc[n] + drecv[n].astype(jnp.float32)
        acc[n] = total
        csend[n] = total.astype(jnp.bfloat16)
        arrive_c2.append(ahead(n, c, sc, csend, crecv, c2s, c2r, 64))
    arrive_b2 = []
    for n in range(CHUNKS):
        for copy in arrive_c2[n]:
            copy.wait_recv()
        total = acc[n, pl.ds(pl.multiple_of(64 * c, 64), 64)]
        for d in range(3):
            total = total + crecv[n, d].astype(jnp.float32)
        bsum[n] = total
        bsend[n] = total.astype(jnp.bfloat16)
        arrive_b2.append(ahead(n, b, sb, bsend, brecv, b2s, b2r, 16))
    arrive_a2 = []
    for n in range(CHUNKS):
        for copy in arrive_b2[n]:
            copy.wait_recv()
        total = bsum[n, rows16(b)]
        for d in range(3):
            total = total + brecv[n, d].astype(jnp.float32)
        fa[n] = total
        for j in range(4):
            piece = fa[n, 4 * j : 4 * j + 4]
            aown[n, j] = piece
            asend[n, j] = piece.astype(jnp.bfloat16)
        copies = []
        for d in (1, 3, 2):
            to, device = ring(a, sa, d)
            k = 3 * n + d - 1
            copies.append(start(asend.at[n, to], arecv.at[n, d - 1], a2s.at[k], a2r.at[k], device))
        arrive_a2.append(copies)
    for n in range(CHUNKS):
        cols = slice(COLS * n, COLS * (n + 1))
        for copy in arrive_a2[n]:
            copy.wait_recv()
        total = hid_ref[:, cols] + aown[n, a]
        for d in range(3):
            total = total + arecv[n, d].astype(jnp.float32)
        out_ref[:, cols] = total.astype(jnp.bfloat16)
    for copy in sends:
        copy.wait_send()


def ffn(x, hidden_state, wg, wu, wd, dg, du, dd):
    bf, f32 = jnp.bfloat16, jnp.float32
    dma = pltpu.SemaphoreType.DMA
    vmem = pl.BlockSpec(memory_space=pltpu.VMEM)
    anywhere = pl.BlockSpec(memory_space=pl.ANY)
    return pl.pallas_call(
        ffn_kernel,
        out_shape=jax.ShapeDtypeStruct((SEQ_DEV, D), bf),
        in_specs=[vmem, vmem, anywhere, anywhere, anywhere, vmem, vmem, vmem],
        out_specs=vmem,
        scratch_shapes=[
            pltpu.VMEM((3, D, 256), bf),
            pltpu.VMEM((512, D), bf),
            pltpu.VMEM((8, 3 * PART, 256), bf),
            pltpu.VMEM((8, 3 * PART, 256), bf),
            pltpu.VMEM((4, 4, WIDE), bf),
            pltpu.VMEM((16, WIDE), f32),
            pltpu.VMEM((256, WIDE), bf),
            pltpu.VMEM((256, WIDE), bf),
            pltpu.VMEM((2, 256, 512), bf),
            pltpu.VMEM((CHUNKS, 256, COLS), f32),
            pltpu.VMEM((CHUNKS, 256, COLS), bf),
            pltpu.VMEM((CHUNKS, 256, COLS), bf),
            pltpu.VMEM((CHUNKS, 256, COLS), bf),
            pltpu.VMEM((CHUNKS, 3, 64, COLS), bf),
            pltpu.VMEM((CHUNKS, 64, COLS), f32),
            pltpu.VMEM((CHUNKS, 64, COLS), bf),
            pltpu.VMEM((CHUNKS, 3, 16, COLS), bf),
            pltpu.VMEM((CHUNKS, 16, COLS), f32),
            pltpu.VMEM((CHUNKS, 4, 4, COLS), f32),
            pltpu.VMEM((CHUNKS, 4, 4, COLS), bf),
            pltpu.VMEM((CHUNKS, 3, 4, COLS), bf),
            dma((7,)), dma((7,)), dma((7,)), dma((3,)), dma((3,)), dma((3,)), dma((3,)),
            dma((12,)), dma((12,)), dma((16,)), dma((16,)),
            dma((CHUNKS,)), dma((CHUNKS,)),
            dma((3 * CHUNKS,)), dma((3 * CHUNKS,)), dma((3 * CHUNKS,)), dma((3 * CHUNKS,)),
            dma((3 * CHUNKS,)), dma((3 * CHUNKS,)),
        ],
        compiler_params=pltpu.CompilerParams(
            collective_id=0, has_side_effects=True, vmem_limit_bytes=48 * 1024 * 1024
        ),
    )(x, hidden_state, wg, wu, wd, dg, du, dd)


def per_device(
    tokens, lengths, cache_keys, cache_values, query_w, key_w, value_w, out_w, mix_lambda, head_gain,
    attn_gain, ffn_gain, routes, route_weights, exp_gate, exp_up, exp_down, dense_gate, dense_up,
    dense_down, branch_gate,
):
    rows = tokens.shape[0]
    groups = HEADS // KV_HEADS
    half = HEAD_DIM // 2
    scale = (HEAD_DIM // 2) ** (-0.5)
    cache_len = cache_keys.shape[1]
    f32 = jnp.float32
    xfull = tokens.astype(f32)
    normed = rms_norm(xfull, attn_gain, 1e-06).astype(jnp.bfloat16)
    query = jnp.dot(normed, query_w, preferred_element_type=f32).astype(jnp.bfloat16)
    key_new = jnp.dot(normed, key_w, preferred_element_type=f32).astype(jnp.bfloat16)
    value_new = jnp.dot(normed, value_w, preferred_element_type=f32).astype(jnp.bfloat16)
    qheads = query.reshape(rows, KV_HEADS, groups, HEAD_DIM)
    knew = key_new.reshape(rows, KV_HEADS, HEAD_DIM)
    vnew = value_new.reshape(rows, KV_HEADS, HEAD_DIM)
    valid = (jnp.arange(cache_len, dtype=jnp.int32)[None, :] < lengths[:, None])[:, None, None, :]
    pairs = []
    for part in (slice(0, half), slice(half, HEAD_DIM)):
        scores = jnp.einsum("sgqd,spgd->sgqp", qheads[..., part], cache_keys[..., part], preferred_element_type=f32)
        own = jnp.einsum("sgqd,sgd->sgq", qheads[..., part], knew[..., part], preferred_element_type=f32)
        pairs.append(softmax_pair(scores * scale, own * scale, valid))
    (prob_one, own_one), (prob_two, own_two) = pairs
    lam = mix_lambda.reshape(KV_HEADS, groups)
    weights = (prob_one - lam[None, :, :, None] * prob_two).astype(jnp.bfloat16)
    own_weights = (own_one - lam[None] * own_two).astype(jnp.bfloat16)
    mixed = jnp.einsum("sgqp,spgd->sgqd", weights, cache_values, preferred_element_type=f32)
    mixed = mixed + own_weights.astype(f32)[..., None] * vnew.astype(f32)[:, :, None, :]
    heads = rms_norm(mixed, head_gain, 1e-05).astype(jnp.bfloat16).reshape(rows, HEADS * HEAD_DIM)
    hidden_state = xfull + jnp.dot(heads, out_w, preferred_element_type=f32)
    ffn_in = rms_norm(hidden_state, ffn_gain, 1e-06).astype(jnp.bfloat16)
    gate = jax.nn.sigmoid(jnp.dot(ffn_in, branch_gate, preferred_element_type=f32))
    match = routes[:, :, None] == jnp.arange(EXPERTS, dtype=jnp.int32)
    weight = jnp.sum(jnp.where(match, route_weights[:, :, None], 0.0), axis=1)
    wide = jnp.concatenate([weight, weight, gate[:, None], gate[:, None]], axis=1)
    high = wide.astype(jnp.bfloat16)
    low = (wide - high.astype(f32)).astype(jnp.bfloat16)
    place = jnp.arange(18)
    side = jnp.where((place < 8) | (place == 16), high, low)
    x = jnp.concatenate([ffn_in, side, jnp.zeros((rows, SIDE - 18), jnp.bfloat16)], axis=1)
    output = ffn(
        x, hidden_state, exp_gate, exp_up, exp_down, dense_gate[0], dense_up[0], dense_down[0]
    )
    return (output, key_new, value_new)


def solution(mesh):
    placed = (
        P("ep", None), P("ep"), P("ep", None, None, None), P("ep", None, None, None),
        P(), P(), P(), P(), P(), P(), P(), P(),
        P("ep", None), P("ep", None), P(None, "ep"), P(None, "ep"), P("ep", None),
        P("ep", None, None), P("ep", None, None), P("ep", None, None), P(),
    )
    return jax.shard_map(
        per_device,
        mesh=mesh,
        in_specs=placed,
        out_specs=(P("ep", None), P("ep", None), P("ep", None)),
        check_vma=False,
    )
```

time: 200 us -> 76 us (0.38)
  waiting for transfers between devices: 66.9 us -> 0 us
  Pallas kernels: 0 us -> 49.8 us
  starting transfers between devices: 41.2 us -> 0 us
  local copies, waits for them, and re-layouts: 37.7 us -> 12.6 us
  other arithmetic: 17.1 us -> 1.69 us
  between operations: 14.5 us -> 0.85 us
  matrix products: 21 us -> 10.7 us
    pallas_call x0 -> x1, Pallas kernels: none -> 49.8 us  [ffn(): pl.pallas_call(ffn_kernel, out_shape=jax.ShapeDtypeStruct((SEQ_DEV, D), b...]
    all_to_all x6 -> x0, waiting for transfers between devices: 48.1 us -> none  [the longest x1 18.7 us: per_device(): lax.all_to_all(outgoing, 'ep', split_axis=0, concat_axis=0, tiled=True)]
    all_to_all x6 -> x0, starting transfers between devices: 41.2 us -> none  [the longest x1 11.9 us: per_device(): lax.all_to_all(outgoing, 'ep', split_axis=0, concat_axis=0, tiled=True)]
    all_gather x1 -> x0, waiting for transfers between devices: 18.9 us -> none  [per_device(): all_rows = lax.all_gather(ffn_in, 'ep', axis=0, tiled=True)]
    dot_general x16 -> x9, matrix products: 20.4 us -> 10.1 us  [the longest x2 3.12 us: per_device(): jnp.einsum('sgqd,spgd->sgqp', qheads[..., part], cache_keys[..., part], p...]
    unnamed x46 -> x44, local copies, waits for them, and re-layouts: 15.6 us -> 5.75 us
    split x2 -> x0, other arithmetic: 9.14 us -> none  [exchange_in_pieces(): jnp.split(tiles, cut_rows(tiles.shape[cut], pieces), axis=cut)]
    split x3 -> x0, local copies, waits for them, and re-layouts: 4.73 us -> none  [the longest x2 3.03 us: exchange_in_pieces(): jnp.split(tiles, cut_rows(tiles.shape[cut], pieces), axis=cut)]
  transfers between devices with their start and end apart: 7 -> 0, of which waited for: 6 -> 0; matrix products, arithmetic and copies ran while one was open for 27% -> 0% of each run, Pallas kernels for 0% -> 0%
where the time goes in v1:
time: 76 us; the launch traced here: 75.6 us
  Pallas kernels  49.8 us (66%)
  local copies, waits for them, and re-layouts  12.6 us (17%)
  matrix products  10.7 us (14%)
  other arithmetic  1.69 us (2%)
  between operations  0.85 us (1%)
    pallas_call x1, Pallas kernels, ffn(): pl.pallas_call(ffn_kernel, out_shape=jax.ShapeDtypeStruct((SEQ_DEV, D), b...  49.8 us
    slice x1, local copies, waits for them, and re-layouts, per_device(): cache_keys[..., part]  6.42 us
    unnamed x44, local copies, waits for them, and re-layouts  5.75 us
    dot_general x2, matrix products, per_device(): jnp.einsum('sgqd,spgd->sgqp', qheads[..., part], cache_keys[..., part], p...  3.12 us
    dot_general x1, matrix products, per_device(): hidden_state = xfull + jnp.dot(heads, out_w, preferred_element_type=f32)  3.03 us
    dot_general x1, matrix products, per_device(): jnp.dot(normed, query_w, preferred_element_type=f32).astype(jnp.bfloat16)  2.92 us

profile of v1, /device:TPU:0, one launch (start us, length us, event | category | flops | bytes accessed | tf_op | source)
XLA Modules:
  0.0 75.6 jit_solution(12884488726827500949)
XLA Ops:
  0.6 0.0 copy-start
  0.6 1.0 %fusion.31 = f32[4]{0:T(128)S(1)} fusion(bf16[4,2048]{1,0:T(4,128)(2,1)} %param.21), kind=kLoop, calls=%fused_computation.36 | loop fusion | flops 24572 | bytes 16400 | tf_op jit(solution)/shard_map/reduce_sum | solution.py:28
  1.7 2.9 %convolution_convert_fusion = bf16[4,1024]{1,0:T(4,128)(2,1)S(1)} fusion(bf16[2048,1024]{1,0:T(8,128)(2,1)} %param.25, bf16[4,2048]{1,0:T(4,128)(2,1)} %param.21, f32[2048]{0:T(1024)} %param.31, f32[4]{0:T(128)S(1)} %add_rsqrt_fusion.2), kind=kOutput, calls=%fused_computation.10 | convolution fusion | flops 16814080 | bytes 4227088 | tf_op jit(solution)/shard_map/dot_general | solution.py:320
  4.6 0.1 iota_compare_fusion
  4.7 6.4 %fusion.50 = (bf16[4,1024,2,64]{3,2,1,0:T(2,128)(2,1)}, bf16[4,1024,2,64]{3,2,1,0:T(2,128)(2,1)S(1)}) fusion(bf16[4,1024,2,128]{3,2,1,0:T(2,128)(2,1)} %param.23), kind=kLoop, calls=%fused_computation.72 | loop fusion | bytes 4194304 | tf_op jit(solution)/shard_map/slice | solution.py:329
  11.1 0.7 select_reduce_fusion.1
  11.9 0.5 copy-done.5
  12.3 0.3 convolution_convert_fusion.2
  12.6 0.1 slice_bitcast_fusion
  12.7 0.1 fusion.37
  12.8 2.4 %fusion.21 = (f32[4,2,4]{2,1,0:T(2,128)S(1)}, f32[4,2,4]{2,1,0:T(2,128)S(1)}, f32[4,2,4,1024]{3,2,1,0:T(4,128)S(1)}) fusion(f32[4,2,4,1024]{3,2,1,0:T(4,128)S(1)} %get-tuple-element.13, f32[4,2,4]{2,1,0:T(2,128)S(1)} %multiply_maximum_fusion.1, pred[4,1024]{1,0:T(4,128)(4,1)S(1)} %iota_compare_fusion, bf16[4,1024,2,64]{3,2,1,0:T(2,128)(2,1)} %get-tuple-element.5, ...), kind=kOutput, calls=%fused_computation.25 | convolution fusion | flops 4390848 | bytes 1323392 | tf_op jit(solution)/shard_map/sgqd,spgd->sgqp/dot_general | solution.py:329
  15.2 0.2 fusion.34
  15.4 0.2 fusion.22
  15.6 0.1 mul.107
  15.8 0.3 convolution_convert_fusion.1
  16.1 0.6 multiply_reduce_fusion.1
  16.7 0.0 copy-done.17
  16.7 0.1 multiply_convert_fusion.1
  16.9 3.0 %multiply_reduce_fusion = (f32[4]{0:T(128)S(1)}, f32[4,2048]{1,0:T(4,128)S(1)}) fusion(bf16[4,1024]{1,0:T(4,128)(2,1)S(1)} %reshape.78, bf16[1024,2048]{1,0:T(8,128)(2,1)} %param.28, bf16[4,2048]{1,0:T(4,128)(2,1)S(1)} %copy-done.7), kind=kOutput, calls=%fused_computation.40 | convolution fusion | flops 16809980 | bytes 4251664 | tf_op jit(solution)/shard_map/dot_general | solution.py:339
  20.0 0.1 multiply_convert_fusion
  20.1 0.1 fusion.19
  20.2 0.1 copy.36
  20.3 0.1 select_reduce_fusion.2
  20.4 0.1 fusion.43
  20.5 0.1 concatenate.7.x_ref
  20.6 0.2 copy.38
  20.8 0.2 copy.39
  21.0 1.4 %copy-done.1 = bf16[2048,384]{1,0:T(8,128)(2,1)S(1)} copy-done((bf16[2048,384]{1,0:T(8,128)(2,1)S(1)}, bf16[2048,384]{1,0:T(8,128)(2,1)}, u32[]{:S(2)}) %copy-start.1) | copy-done | bytes 1572888
  22.4 1.4 %copy-done.2 = bf16[2048,384]{1,0:T(8,128)(2,1)S(1)} copy-done((bf16[2048,384]{1,0:T(8,128)(2,1)S(1)}, bf16[2048,384]{1,0:T(8,128)(2,1)}, u32[]{:S(2)}) %copy-start.2) | copy-done | bytes 1572888
  23.8 1.4 %copy-done.3 = bf16[384,2048]{1,0:T(8,128)(2,1)S(1)} copy-done((bf16[384,2048]{1,0:T(8,128)(2,1)S(1)}, bf16[384,2048]{1,0:T(8,128)(2,1)}, u32[]{:S(2)}) %copy-start.3) | copy-done | bytes 1572888
  25.2 49.8 %shard_map.220 = bf16[4,2048]{1,0:T(4,128)(2,1)S(1)} custom-call(bf16[4,2176]{1,0:T(4,128)(2,1)S(1)} %concatenate.7.x_ref, f32[4,2048]{1,0:T(4,128)S(1)} %get-tuple-element.18.hid_ref, bf16[2048,384]{1,0:T(8,128)(2,1)S(1)} %copy-done.1, bf16[2048,384]{1,0:T(8,128)(2,1)S(1)} %copy-done.2, bf16[384,2048]{1,0:T(8,128)(2,1)S(1)} %copy-done.3, ...), custom_call_target="tpu_custom_call" | custom-call | tf_op jit(solution)/shard_map/pallas_call | solution.py:268
  75.0 0.6 copy.69
  (47 shorter events, 0.2 us)
Async XLA Ops:
  0.6 15.4 %copy-start = (bf16[4,1024,2,128]{3,2,1,0:T(2,128)(2,1)S(1)}, bf16[4,1024,2,128]{3,2,1,0:T(2,128)(2,1)}, u32[]{:S(2)}) copy-start(bf16[4,1024,2,128]{3,2,1,0:T(2,128)(2,1)} %param.24) | copy-start | bytes 6291460
  1.7 2.9 %copy-start.18 = (s32[4]{0:T(128)S(1)}, s32[4]{0:T(128)}, u32[]{:S(2)}) copy-start(s32[4]{0:T(128)} %param.22) | copy-start | bytes 52
  11.1 1.2 %copy-start.5 = (bf16[2048,256]{1,0:T(8,128)(2,1)S(1)}, bf16[2048,256]{1,0:T(8,128)(2,1)}, u32[]{:S(2)}) copy-start(bf16[2048,256]{1,0:T(8,128)(2,1)} %param.26) | copy-start | bytes 3145732
  11.1 1.2 %copy-start.7 = (bf16[4,2048]{1,0:T(4,128)(2,1)S(1)}, bf16[4,2048]{1,0:T(4,128)(2,1)}, u32[]{:S(2)}) copy-start(bf16[4,2048]{1,0:T(4,128)(2,1)} %param.21) | copy-start | bytes 49156
  11.1 1.2 %copy-start.10 = (f32[2048]{0:T(1024)S(1)}, f32[2048]{0:T(1024)}, u32[]{:S(2)}) copy-start(f32[2048]{0:T(1024)} %param.31) | copy-start | bytes 24580
  11.9 3.8 %copy-start.19 = (f32[8]{0:T(128)S(1)}, f32[8]{0:T(128)}, u32[]{:S(2)}) copy-start(f32[8]{0:T(128)} %param.29) | copy-start | bytes 100
  11.9 3.9 %copy-start.6 = (bf16[2048,256]{1,0:T(8,128)(2,1)S(1)}, bf16[2048,256]{1,0:T(8,128)(2,1)}, u32[]{:S(2)}) copy-start(bf16[2048,256]{1,0:T(8,128)(2,1)} %param.27) | copy-start | bytes 3145732
  12.6 4.1 %copy-start.12 = (bf16[4,256]{1,0:T(4,128)(2,1)}, bf16[4,256]{1,0:T(4,128)(2,1)S(1)}, u32[]{:S(2)}) copy-start(bf16[4,256]{1,0:T(4,128)(2,1)S(1)} %convolution_convert_fusion.2) | copy-start | bytes 6148
  16.1 0.6 copy-start.11
  16.1 0.7 copy-start.17
  16.8 3.1 %copy-start.13 = (f32[2048]{0:T(1024)S(1)}, f32[2048]{0:T(1024)}, u32[]{:S(2)}) copy-start(f32[2048]{0:T(1024)} %param.32) | copy-start | bytes 24580
  16.8 3.2 %copy-start.14 = (bf16[2048]{0:T(1024)(128)(2,1)S(1)}, bf16[2048]{0:T(1024)(128)(2,1)}, u32[]{:S(2)}) copy-start(bf16[2048]{0:T(1024)(128)(2,1)} %param.41) | copy-start | bytes 12292
  16.8 3.4 %copy-start.15 = (f32[4,2]{0,1:T(2,128)S(1)}, f32[4,2]{0,1:T(2,128)}, u32[]{:S(2)}) copy-start(f32[4,2]{0,1:T(2,128)} %param.34) | copy-start | bytes 100
  16.9 3.4 %copy-start.16 = (s32[4,2]{0,1:T(2,128)S(1)}, s32[4,2]{0,1:T(2,128)}, u32[]{:S(2)}) copy-start(s32[4,2]{0,1:T(2,128)} %param.33) | copy-start | bytes 100
  16.9 3.7 %copy-start.8 = (bf16[1,256,352]{1,2,0:T(8,128)(2,1)S(1)}, bf16[1,256,352]{1,2,0:T(8,128)(2,1)}, u32[]{:S(2)}) copy-start(bf16[1,256,352]{1,2,0:T(8,128)(2,1)} %param.38) | copy-start | bytes 540676
  16.9 3.9 %copy-start.9 = (bf16[1,256,352]{1,2,0:T(8,128)(2,1)S(1)}, bf16[1,256,352]{1,2,0:T(8,128)(2,1)}, u32[]{:S(2)}) copy-start(bf16[1,256,352]{1,2,0:T(8,128)(2,1)} %param.39) | copy-start | bytes 540676
  16.9 4.0 %copy-start.4 = (bf16[1,352,256]{2,1,0:T(8,128)(2,1)S(1)}, bf16[1,352,256]{2,1,0:T(8,128)(2,1)}, u32[]{:S(2)}) copy-start(bf16[1,352,256]{2,1,0:T(8,128)(2,1)} %param.40) | copy-start | bytes 540676
  20.9 1.4 %copy-start.1 = (bf16[2048,384]{1,0:T(8,128)(2,1)S(1)}, bf16[2048,384]{1,0:T(8,128)(2,1)}, u32[]{:S(2)}) copy-start(bf16[2048,384]{1,0:T(8,128)(2,1)} %wg_hbm.1) | copy-start | bytes 4718596
  22.4 1.4 %copy-start.2 = (bf16[2048,384]{1,0:T(8,128)(2,1)S(1)}, bf16[2048,384]{1,0:T(8,128)(2,1)}, u32[]{:S(2)}) copy-start(bf16[2048,384]{1,0:T(8,128)(2,1)} %wu_hbm.1) | copy-start | bytes 4718596
  23.8 1.4 %copy-start.3 = (bf16[384,2048]{1,0:T(8,128)(2,1)S(1)}, bf16[384,2048]{1,0:T(8,128)(2,1)}, u32[]{:S(2)}) copy-start(bf16[384,2048]{1,0:T(8,128)(2,1)} %wd_hbm.1) | copy-start | bytes 4718596

commit v2 on v1

--- a/solution.py
+++ b/solution.py
@@ -1,5 +1,3 @@
-import functools
-
 import jax
 import jax.numpy as jnp
 from jax import lax
@@ -11,14 +9,15 @@
 KV_HEADS = 2
 HEAD_DIM = 128
 SEQ_DEV = 4
+CACHE = 1024
 SPLIT = 16
-EXPERTS = 8
 D = 2048
 SIDE = 128
 WIDE = D + SIDE
 HID = 384
 PART = 48
 CHUNKS = 4
+VMEM_LIMIT = 67043328
 COLS = D // CHUNKS
 MESH = pl.DeviceIdType.MESH
 NT = (((1,), (1,)), ((), ()))
@@ -27,15 +26,6 @@
 def rms_norm(values, gain, epsilon):
     scale = lax.rsqrt(jnp.mean(values * values, axis=-1, keepdims=True) + epsilon)
     return values * scale * gain
-
-
-def softmax_pair(scores, own_score, valid):
-    masked = jnp.where(valid, scores, -jnp.inf)
-    largest = jnp.maximum(jnp.max(masked, axis=-1), own_score)
-    raised = jnp.where(valid, jnp.exp(scores - largest[..., None]), 0.0)
-    own_raised = jnp.exp(own_score - largest)
-    total = jnp.sum(raised, axis=-1) + own_raised
-    return (raised / total[..., None], own_raised / total)
 
 
 def remote(src, dst, send, recv, device):
@@ -49,11 +39,15 @@
     return pl.ds(pl.multiple_of(block * 16, 16), count)
 
 
-def ffn_kernel(
-    x_ref, hid_ref, wg_hbm, wu_hbm, wd_hbm, dg_ref, du_ref, dd_ref,
-    out_ref,
+def layer_kernel(
+    len_ref, lam_ref, routes_ref, rweights_ref, tok_ref, again_ref, fgain_ref, hgain_ref, bgate_ref,
+    keys_hbm, values_hbm, qw_hbm, kw_hbm, vw_hbm, ow_hbm,
+    wg_hbm, wu_hbm, wd_hbm, dg_hbm, du_hbm, dd_hbm,
+    out_ref, newk_ref, newv_ref,
+    keys, values, qw, kvw, ow, dg_ref, du_ref, dd_ref, qf, qs, hf, hid_ref, x_ref,
     wgu, wdx, wsend, wrecv, own4, pack, xown, xpart, act, acc, psend, drecv, csend, crecv,
     bsum, bsend, brecv, fa, aown, asend, arecv,
+    dsem, qsem, ksem, vsem, osem,
     wsem, rs_w, rr_w, as_s, as_r, bs_s, bs_r, cs_s, cs_r, ds_s, ds_r,
     d2s, d2r, c2s, c2r, b2s, b2r, a2s, a2r,
 ):
@@ -77,14 +71,26 @@
         new = lax.rem(row_block + d, 8)
         return new, me + (new - row_block) * SPLIT
 
-    loads = []
-    for n in range(3):
-        cols = pl.ds(128 * n, 128)
-        loads.append(pltpu.make_async_copy(wg_hbm.at[:, cols], wgu.at[n, :, pl.ds(0, 128)], wsem.at[2 * n]))
-        loads.append(pltpu.make_async_copy(wu_hbm.at[:, cols], wgu.at[n, :, pl.ds(128, 128)], wsem.at[2 * n + 1]))
-    loads.append(pltpu.make_async_copy(wd_hbm, wdx.at[pl.ds(0, HID)], wsem.at[6]))
-    for load in loads:
-        load.start()
+    bf, f32 = jnp.bfloat16, jnp.float32
+
+    def fetch(src, dst, sem):
+        copy = pltpu.make_async_copy(src, dst, sem)
+        copy.start()
+        return copy
+
+    dense_in = [fetch(dg_hbm, dg_ref, dsem.at[0]), fetch(du_hbm, du_ref, dsem.at[1]), fetch(dd_hbm, dd_ref, dsem.at[2])]
+    proj_in = []
+    for n in range(4):
+        cols = pl.ds(256 * n, 256)
+        proj_in.append(fetch(qw_hbm.at[:, cols], qw.at[:, cols], qsem.at[n]))
+    proj_in.append(fetch(kw_hbm, kvw.at[:, pl.ds(0, 256)], qsem.at[4]))
+    proj_in.append(fetch(vw_hbm, kvw.at[:, pl.ds(256, 256)], qsem.at[5]))
+    span = [pl.ds(2 * CACHE * s, 2 * CACHE) for s in range(SEQ_DEV)]
+    keys_in = [fetch(keys_hbm.at[span[s]], keys.at[s], ksem.at[s]) for s in range(SEQ_DEV)]
+    values_in = [fetch(values_hbm.at[span[s]], values.at[s], vsem.at[s]) for s in range(SEQ_DEV)]
+    out_in = [
+        fetch(ow_hbm.at[:, pl.ds(512 * n, 512)], ow.at[:, pl.ds(512 * n, 512)], osem.at[n]) for n in range(4)
+    ]
 
     barrier = pltpu.get_barrier_semaphore()
     for coord, stride in ((a, sa), (b, sb), (c, sc)):
@@ -93,7 +99,6 @@
     for d in range(1, 8):
         pl.semaphore_signal(barrier, inc=1, device_id=(group(d)[1],), device_id_type=MESH)
     pl.semaphore_signal(barrier, inc=1, device_id=(partner,), device_id_type=MESH)
-    pl.semaphore_wait(barrier, 17)
 
     sends = []
 
@@ -103,28 +108,110 @@
         sends.append(copy)
         return copy
 
-    arrive_a = [start(x_ref, own4.at[a], as_s.at[d], as_r.at[d], ring(a, sa, d + 1)[1]) for d in range(3)]
-    own4[a] = x_ref[...]
-
-    eye = (
-        lax.broadcasted_iota(jnp.int32, (384, 352), 0) == lax.broadcasted_iota(jnp.int32, (384, 352), 1)
-    ).astype(jnp.bfloat16)
-    gate_t = lax.dot_general(eye, dg_ref[...], NT, preferred_element_type=jnp.float32).astype(jnp.bfloat16)
-    up_t = lax.dot_general(eye, du_ref[...], NT, preferred_element_type=jnp.float32).astype(jnp.bfloat16)
-    for r in range(8):
-        wsend[r, 0:PART] = gate_t[PART * r : PART * (r + 1)]
-        wsend[r, PART : 2 * PART] = up_t[PART * r : PART * (r + 1)]
-        if r < 7:
-            wsend[r, 2 * PART :] = dd_ref[PART * r : PART * (r + 1)]
-        else:
-            wsend[r, 2 * PART : 2 * PART + 16] = dd_ref[336:352]
-            wsend[r, 2 * PART + 16 :] = jnp.zeros((32, 256), jnp.bfloat16)
+    for copy in dense_in:
+        copy.wait()
+    for k, tile in enumerate((dg_ref, du_ref, dd_ref)):
+        for r in range(7):
+            wsend[r, PART * k : PART * (k + 1)] = tile[PART * r : PART * (r + 1)]
+        wsend[7, PART * k : PART * k + 16] = tile[336:352]
+        wsend[7, PART * k + 16 : PART * (k + 1)] = jnp.zeros((32, 256), bf)
+    pl.semaphore_wait(barrier, 17)
     arrive_w = []
     for d in range(7):
         to, device = group(d + 1)
         arrive_w.append(start(wsend.at[to], wrecv.at[row_block], rs_w.at[d], rr_w.at[d], device))
     wrecv[row_block] = wsend[row_block]
 
+
+    normed = rms_norm(tok_ref[...].astype(f32), again_ref[...], 1e-06).astype(bf)
+    for n in range(4):
+        proj_in[n].wait()
+        cols = slice(256 * n, 256 * (n + 1))
+        qf[:, cols] = jnp.dot(normed, qw[:, cols], preferred_element_type=f32).astype(bf).astype(f32)
+    proj_in[4].wait()
+    proj_in[5].wait()
+    new = jnp.dot(normed, kvw[...], preferred_element_type=f32).astype(bf)
+    newk_ref[...] = new[:, :256]
+    newv_ref[...] = new[:, 256:]
+    qf[:, HEADS * HEAD_DIM :] = new.astype(f32)
+    for s in range(SEQ_DEV):
+        for h in range(HEADS):
+            qs[s, h : h + 1] = qf[s : s + 1, HEAD_DIM * h : HEAD_DIM * (h + 1)]
+
+    loads = []
+    for n in range(3):
+        cols = pl.ds(128 * n, 128)
+        loads.append(fetch(wg_hbm.at[:, cols], wgu.at[n, :, pl.ds(0, 128)], wsem.at[2 * n]))
+        loads.append(fetch(wu_hbm.at[:, cols], wgu.at[n, :, pl.ds(128, 128)], wsem.at[2 * n + 1]))
+    loads.append(fetch(wd_hbm, wdx.at[pl.ds(0, HID)], wsem.at[6]))
+
+    head8 = lax.broadcasted_iota(jnp.int32, (HEADS, HEAD_DIM), 0)
+    lane8 = lax.broadcasted_iota(jnp.int32, (HEADS, HEAD_DIM), 1)
+    low_head, low_lane = head8 < HEADS // KV_HEADS, lane8 < HEAD_DIM // 2
+    head1 = lax.broadcasted_iota(jnp.int32, (HEADS, 1), 0)
+    lam = jnp.zeros((HEADS, 1), f32)
+    for h in range(HEADS):
+        lam = jnp.where(head1 == h, lam_ref[h], lam)
+    slot = lax.broadcasted_iota(jnp.int32, (HEADS, 2 * CACHE), 1)
+    kv_of = lax.broadcasted_iota(jnp.int32, (HEADS, 2 * CACHE), 0) // (HEADS // KV_HEADS)
+    mine_kv = (slot & 1) == kv_of
+    scale = (HEAD_DIM // 2) ** (-0.5)
+
+    def probabilities(scores, own, valid):
+        largest = jnp.maximum(jnp.max(jnp.where(valid, scores, -jnp.inf), axis=1, keepdims=True), own)
+        raised = jnp.where(valid, jnp.exp(scores - largest), 0.0)
+        own_raised = jnp.exp(own - largest)
+        total = jnp.sum(raised, axis=1, keepdims=True) + own_raised
+        return raised, own_raised, 1.0 / total
+
+    base = HEADS * HEAD_DIM
+    for s in range(SEQ_DEV):
+        q = qs[s]
+        q_one, q_two = jnp.where(low_lane, q, 0.0), jnp.where(low_lane, 0.0, q)
+        rows = [qf[s : s + 1, base + 128 * k : base + 128 * (k + 1)] for k in range(4)]
+        own_key = jnp.where(low_head, rows[0], rows[1])
+        own_value = jnp.where(low_head, rows[2], rows[3])
+        own_one = jnp.sum(q_one * own_key, axis=1, keepdims=True) * scale
+        own_two = jnp.sum(q_two * own_key, axis=1, keepdims=True) * scale
+        keys_in[s].wait()
+        both = jnp.concatenate([q_one, q_two], axis=0).astype(bf)
+        scores = lax.dot_general(both, keys[s], NT, preferred_element_type=f32) * scale
+        valid = mine_kv & (slot < 2 * len_ref[s])
+        raised_one, own_one, inv_one = probabilities(scores[:HEADS], own_one, valid)
+        raised_two, own_two, inv_two = probabilities(scores[HEADS:], own_two, valid)
+        inv_two = inv_two * lam
+        weights = (raised_one * inv_one - raised_two * inv_two).astype(bf)
+        own_weight = (own_one * inv_one - own_two * inv_two).astype(bf).astype(f32)
+        values_in[s].wait()
+        mixed = jnp.dot(weights, values[s], preferred_element_type=f32) + own_weight * own_value
+        mixed = rms_norm(mixed, hgain_ref[...], 1e-05)
+        for h in range(HEADS):
+            hf[s : s + 1, HEAD_DIM * h : HEAD_DIM * (h + 1)] = mixed[h : h + 1]
+    heads = hf[...].astype(bf)
+    for n in range(4):
+        out_in[n].wait()
+        cols = slice(512 * n, 512 * (n + 1))
+        hid_ref[:, cols] = tok_ref[:, cols].astype(f32) + jnp.dot(heads, ow[:, cols], preferred_element_type=f32)
+    ffn_in = rms_norm(hid_ref[...], fgain_ref[...], 1e-06).astype(bf)
+    gate_row = bgate_ref[...].astype(f32)
+    terms = jnp.zeros((SEQ_DEV, 128), f32)
+    for k in range(16):
+        terms = terms + ffn_in[:, 128 * k : 128 * (k + 1)].astype(f32) * gate_row[k : k + 1]
+    gate = jax.nn.sigmoid(jnp.sum(terms, axis=1, keepdims=True))
+    place = lax.broadcasted_iota(jnp.int32, (SEQ_DEV, SIDE), 1)
+    row = lax.broadcasted_iota(jnp.int32, (SEQ_DEV, SIDE), 0)
+    full = jnp.where((place == 16) | (place == 17), gate, 0.0)
+    for t in range(SEQ_DEV):
+        for k in range(2):
+            chosen = (row == t) & (place < 16) & ((place & 7) == routes_ref[k, t])
+            full = full + jnp.where(chosen, rweights_ref[k, t], 0.0)
+    high = full.astype(bf).astype(f32)
+    side = jnp.where((place < 8) | (place == 16), high, full - high)
+    x_ref[:, :D] = ffn_in
+    x_ref[:, D:] = side.astype(bf)
+
+    arrive_a = [start(x_ref, own4.at[a], as_s.at[d], as_r.at[d], ring(a, sa, d + 1)[1]) for d in range(3)]
+    own4[a] = x_ref[...]
     for copy in arrive_a:
         copy.wait_recv()
     for j in range(4):
@@ -260,17 +347,40 @@
         copy.wait_send()
 
 
-def ffn(x, hidden_state, wg, wu, wd, dg, du, dd):
+def per_device(
+    tokens, lengths, cache_keys, cache_values, query_w, key_w, value_w, out_w, mix_lambda, head_gain,
+    attn_gain, ffn_gain, routes, route_weights, exp_gate, exp_up, exp_down, dense_gate, dense_up,
+    dense_down, branch_gate,
+):
     bf, f32 = jnp.bfloat16, jnp.float32
     dma = pltpu.SemaphoreType.DMA
     vmem = pl.BlockSpec(memory_space=pltpu.VMEM)
+    smem = pl.BlockSpec(memory_space=pltpu.SMEM)
     anywhere = pl.BlockSpec(memory_space=pl.ANY)
+    kv = KV_HEADS * HEAD_DIM
     return pl.pallas_call(
-        ffn_kernel,
-        out_shape=jax.ShapeDtypeStruct((SEQ_DEV, D), bf),
-        in_specs=[vmem, vmem, anywhere, anywhere, anywhere, vmem, vmem, vmem],
-        out_specs=vmem,
+        layer_kernel,
+        out_shape=(
+            jax.ShapeDtypeStruct((SEQ_DEV, D), bf),
+            jax.ShapeDtypeStruct((SEQ_DEV, kv), bf),
+            jax.ShapeDtypeStruct((SEQ_DEV, kv), bf),
+        ),
+        in_specs=[smem] * 4 + [vmem] * 5 + [anywhere] * 12,
+        out_specs=(vmem, vmem, vmem),
         scratch_shapes=[
+            pltpu.VMEM((SEQ_DEV, 2 * CACHE, HEAD_DIM), bf),
+            pltpu.VMEM((SEQ_DEV, 2 * CACHE, HEAD_DIM), bf),
+            pltpu.VMEM((D, HEADS * HEAD_DIM), bf),
+            pltpu.VMEM((D, 2 * kv), bf),
+            pltpu.VMEM((HEADS * HEAD_DIM, D), bf),
+            pltpu.VMEM((352, 256), bf),
+            pltpu.VMEM((352, 256), bf),
+            pltpu.VMEM((352, 256), bf),
+            pltpu.VMEM((SEQ_DEV, HEADS * HEAD_DIM + 2 * kv), f32),
+            pltpu.VMEM((SEQ_DEV, HEADS, HEAD_DIM), f32),
+            pltpu.VMEM((SEQ_DEV, HEADS * HEAD_DIM), f32),
+            pltpu.VMEM((SEQ_DEV, D), f32),
+            pltpu.VMEM((SEQ_DEV, WIDE), bf),
             pltpu.VMEM((3, D, 256), bf),
             pltpu.VMEM((512, D), bf),
             pltpu.VMEM((8, 3 * PART, 256), bf),
@@ -292,6 +402,7 @@
             pltpu.VMEM((CHUNKS, 4, 4, COLS), f32),
             pltpu.VMEM((CHUNKS, 4, 4, COLS), bf),
             pltpu.VMEM((CHUNKS, 3, 4, COLS), bf),
+            dma((3,)), dma((6,)), dma((4,)), dma((4,)), dma((4,)),
             dma((7,)), dma((7,)), dma((7,)), dma((3,)), dma((3,)), dma((3,)), dma((3,)),
             dma((12,)), dma((12,)), dma((16,)), dma((16,)),
             dma((CHUNKS,)), dma((CHUNKS,)),
@@ -299,58 +410,14 @@
             dma((3 * CHUNKS,)), dma((3 * CHUNKS,)),
         ],
         compiler_params=pltpu.CompilerParams(
-            collective_id=0, has_side_effects=True, vmem_limit_bytes=48 * 1024 * 1024
+            collective_id=0, has_side_effects=True, vmem_limit_bytes=VMEM_LIMIT
         ),
-    )(x, hidden_state, wg, wu, wd, dg, du, dd)
-
-
-def per_device(
-    tokens, lengths, cache_keys, cache_values, query_w, key_w, value_w, out_w, mix_lambda, head_gain,
-    attn_gain, ffn_gain, routes, route_weights, exp_gate, exp_up, exp_down, dense_gate, dense_up,
-    dense_down, branch_gate,
-):
-    rows = tokens.shape[0]
-    groups = HEADS // KV_HEADS
-    half = HEAD_DIM // 2
-    scale = (HEAD_DIM // 2) ** (-0.5)
-    cache_len = cache_keys.shape[1]
-    f32 = jnp.float32
-    xfull = tokens.astype(f32)
-    normed = rms_norm(xfull, attn_gain, 1e-06).astype(jnp.bfloat16)
-    query = jnp.dot(normed, query_w, preferred_element_type=f32).astype(jnp.bfloat16)
-    key_new = jnp.dot(normed, key_w, preferred_element_type=f32).astype(jnp.bfloat16)
-    value_new = jnp.dot(normed, value_w, preferred_element_type=f32).astype(jnp.bfloat16)
-    qheads = query.reshape(rows, KV_HEADS, groups, HEAD_DIM)
-    knew = key_new.reshape(rows, KV_HEADS, HEAD_DIM)
-    vnew = value_new.reshape(rows, KV_HEADS, HEAD_DIM)
-    valid = (jnp.arange(cache_len, dtype=jnp.int32)[None, :] < lengths[:, None])[:, None, None, :]
-    pairs = []
-    for part in (slice(0, half), slice(half, HEAD_DIM)):
-        scores = jnp.einsum("sgqd,spgd->sgqp", qheads[..., part], cache_keys[..., part], preferred_element_type=f32)
-        own = jnp.einsum("sgqd,sgd->sgq", qheads[..., part], knew[..., part], preferred_element_type=f32)
-        pairs.append(softmax_pair(scores * scale, own * scale, valid))
-    (prob_one, own_one), (prob_two, own_two) = pairs
-    lam = mix_lambda.reshape(KV_HEADS, groups)
-    weights = (prob_one - lam[None, :, :, None] * prob_two).astype(jnp.bfloat16)
-    own_weights = (own_one - lam[None] * own_two).astype(jnp.bfloat16)
-    mixed = jnp.einsum("sgqp,spgd->sgqd", weights, cache_values, preferred_element_type=f32)
-    mixed = mixed + own_weights.astype(f32)[..., None] * vnew.astype(f32)[:, :, None, :]
-    heads = rms_norm(mixed, head_gain, 1e-05).astype(jnp.bfloat16).reshape(rows, HEADS * HEAD_DIM)
-    hidden_state = xfull + jnp.dot(heads, out_w, preferred_element_type=f32)
-    ffn_in = rms_norm(hidden_state, ffn_gain, 1e-06).astype(jnp.bfloat16)
-    gate = jax.nn.sigmoid(jnp.dot(ffn_in, branch_gate, preferred_element_type=f32))
-    match = routes[:, :, None] == jnp.arange(EXPERTS, dtype=jnp.int32)
-    weight = jnp.sum(jnp.where(match, route_weights[:, :, None], 0.0), axis=1)
-    wide = jnp.concatenate([weight, weight, gate[:, None], gate[:, None]], axis=1)
-    high = wide.astype(jnp.bfloat16)
-    low = (wide - high.astype(f32)).astype(jnp.bfloat16)
-    place = jnp.arange(18)
-    side = jnp.where((place < 8) | (place == 16), high, low)
-    x = jnp.concatenate([ffn_in, side, jnp.zeros((rows, SIDE - 18), jnp.bfloat16)], axis=1)
-    output = ffn(
-        x, hidden_state, exp_gate, exp_up, exp_down, dense_gate[0], dense_up[0], dense_down[0]
+    )(
+        lengths, mix_lambda, routes.T, route_weights.T, tokens, attn_gain.reshape(1, D), ffn_gain.reshape(1, D), head_gain.reshape(1, HEAD_DIM),
+        branch_gate.reshape(16, 128),
+        cache_keys.reshape(-1, HEAD_DIM), cache_values.reshape(-1, HEAD_DIM), query_w, key_w, value_w, out_w,
+        exp_gate, exp_up, exp_down, dense_gate[0].T, dense_up[0].T, dense_down[0],
     )
-    return (output, key_new, value_new)
 
 
 def solution(mesh):

time: 76 us -> 58.7 us (0.77)
  matrix products: 10.7 us -> 0 us
  local copies, waits for them, and re-layouts: 12.6 us -> 3.81 us
  Pallas kernels: 49.8 us -> 54 us
  other arithmetic: 1.69 us -> 0 us
    dot_general x10 -> x0, matrix products: 10.7 us -> none  [the longest x2 3.12 us: per_device(): jnp.einsum('sgqd,spgd->sgqp', qheads[..., part], cache_keys[..., part], p...]
    slice x2 -> x0, local copies, waits for them, and re-layouts: 6.5 us -> none  [the longest x1 6.42 us: per_device(): cache_keys[..., part]]
    pallas_call x1, Pallas kernels: 49.8 us -> 54 us  [per_device(): pl.pallas_call(layer_kernel, out_shape=(jax.ShapeDtypeStruct((SEQ_DEV, D)...]
    unnamed x44 -> x3, local copies, waits for them, and re-layouts: 5.75 us -> 3.81 us
    reduce_sum x3 -> x0, other arithmetic: 1.31 us -> none  [the longest x1 1 us: rms_norm(): jnp.mean(values * values, axis=-1, keepdims=True) + epsilon]
where the time goes in v2:
time: 58.7 us; the launch traced here: 58.4 us
  Pallas kernels  54 us (92%)
  local copies, waits for them, and re-layouts  3.81 us (6%)
  between operations  0.65 us (1%)
    pallas_call x1, Pallas kernels, per_device(): pl.pallas_call(layer_kernel, out_shape=(jax.ShapeDtypeStruct((SEQ_DEV, D)...  54 us
    unnamed x3, local copies, waits for them, and re-layouts  3.81 us

profile of v2, /device:TPU:0, one launch (start us, length us, event | category | flops | bytes accessed | tf_op | source)
XLA Modules:
  0.0 58.4 jit_solution(7677350528041520482)
XLA Ops:
  0.6 54.0 %shard_map.220 = (bf16[4,2048]{1,0:T(4,128)(2,1)}, bf16[4,256]{1,0:T(4,128)(2,1)}, bf16[4,256]{1,0:T(4,128)(2,1)}) custom-call(s32[4]{0:T(128)} %len_ref.1, f32[8]{0:T(128)} %lam_ref.1, s32[2,4]{1,0:T(2,128)} %bitcast.23, f32[2,4]{1,0:T(2,128)} %bitcast.24, bf16[4,2048]{1,0:T(4,128)(2,1)} %tok_ref.1, f32[1,2048]{1,0:T(1,128)} %bitcast.20, ...), custom_call_target="tpu_custom_call" | custom-call | tf_op jit(solution)/shard_map/pallas_call | solution.py:361
  54.6 1.3 %copy.27 = bf16[4,2048]{1,0:T(4,128)(2,1)} copy(bf16[4,2048]{1,0:T(4,128)(2,1)} %get-tuple-element.6) | data formatting | bytes 32768
  56.0 1.2 %copy.28 = bf16[4,256]{1,0:T(4,128)(2,1)} copy(bf16[4,256]{1,0:T(4,128)(2,1)} %get-tuple-element.7) | data formatting | bytes 4096
  57.2 1.2 %copy.29 = bf16[4,256]{1,0:T(4,128)(2,1)} copy(bf16[4,256]{1,0:T(4,128)(2,1)} %get-tuple-element.8) | data formatting | bytes 4096

commit v3 on v2

--- a/solution.py
+++ b/solution.py
@@ -17,7 +17,7 @@
 HID = 384
 PART = 48
 CHUNKS = 4
-VMEM_LIMIT = 67043328
+VMEM_LIMIT = 67043328 - 131072
 COLS = D // CHUNKS
 MESH = pl.DeviceIdType.MESH
 NT = (((1,), (1,)), ((), ()))
@@ -40,14 +40,15 @@
 
 
 def layer_kernel(
-    len_ref, lam_ref, routes_ref, rweights_ref, tok_ref, again_ref, fgain_ref, hgain_ref, bgate_ref,
+    len_hbm, lam_hbm, routes_hbm, rweights_hbm, tok_hbm, again_hbm, fgain_hbm, hgain_hbm, bgate_hbm,
     keys_hbm, values_hbm, qw_hbm, kw_hbm, vw_hbm, ow_hbm,
     wg_hbm, wu_hbm, wd_hbm, dg_hbm, du_hbm, dd_hbm,
     out_ref, newk_ref, newv_ref,
-    keys, values, qw, kvw, ow, dg_ref, du_ref, dd_ref, qf, qs, hf, hid_ref, x_ref,
+    len_ref, lam_ref, routes_ref, rweights_ref, tok_ref, again_ref, fgain_ref, hgain_ref, bgate_ref,
+    keys, values, qw, kvw, ow, dg_ref, du_ref, dd_ref, qf, qs, sc, hf, hid_ref, x_ref,
     wgu, wdx, wsend, wrecv, own4, pack, xown, xpart, act, acc, psend, drecv, csend, crecv,
     bsum, bsend, brecv, fa, aown, asend, arecv,
-    dsem, qsem, ksem, vsem, osem,
+    isem, dsem, qsem, ksem, vsem, osem,
     wsem, rs_w, rr_w, as_s, as_r, bs_s, bs_r, cs_s, cs_r, ds_s, ds_r,
     d2s, d2r, c2s, c2r, b2s, b2r, a2s, a2r,
 ):
@@ -59,7 +60,7 @@
     other = 1 - core
     a, sa = x * other + y * core, 2 * other + 8 * core
     b, sb = y * other + z * core, 8 * other + 32 * core
-    c, sc = z * other + x * core, 32 * other + 2 * core
+    c, sc_ = z * other + x * core, 32 * other + 2 * core
     row_block = lax.div(me, SPLIT)
     partner = me + other - core
 
@@ -78,22 +79,25 @@
         copy.start()
         return copy
 
-    dense_in = [fetch(dg_hbm, dg_ref, dsem.at[0]), fetch(du_hbm, du_ref, dsem.at[1]), fetch(dd_hbm, dd_ref, dsem.at[2])]
+    small = (
+        (tok_hbm, tok_ref), (again_hbm, again_ref), (len_hbm, len_ref), (lam_hbm, lam_ref),
+        (routes_hbm, routes_ref), (rweights_hbm, rweights_ref), (fgain_hbm, fgain_ref),
+        (hgain_hbm, hgain_ref), (bgate_hbm, bgate_ref),
+    )
+    small_in = [fetch(src, dst, isem.at[k]) for k, (src, dst) in enumerate(small)]
+    dense_in = [
+        fetch(src, dst, dsem.at[k])
+        for k, (src, dst) in enumerate(((dg_hbm, dg_ref), (du_hbm, du_ref), (dd_hbm, dd_ref)))
+    ]
     proj_in = []
     for n in range(4):
         cols = pl.ds(256 * n, 256)
         proj_in.append(fetch(qw_hbm.at[:, cols], qw.at[:, cols], qsem.at[n]))
     proj_in.append(fetch(kw_hbm, kvw.at[:, pl.ds(0, 256)], qsem.at[4]))
     proj_in.append(fetch(vw_hbm, kvw.at[:, pl.ds(256, 256)], qsem.at[5]))
-    span = [pl.ds(2 * CACHE * s, 2 * CACHE) for s in range(SEQ_DEV)]
-    keys_in = [fetch(keys_hbm.at[span[s]], keys.at[s], ksem.at[s]) for s in range(SEQ_DEV)]
-    values_in = [fetch(values_hbm.at[span[s]], values.at[s], vsem.at[s]) for s in range(SEQ_DEV)]
-    out_in = [
-        fetch(ow_hbm.at[:, pl.ds(512 * n, 512)], ow.at[:, pl.ds(512 * n, 512)], osem.at[n]) for n in range(4)
-    ]
 
     barrier = pltpu.get_barrier_semaphore()
-    for coord, stride in ((a, sa), (b, sb), (c, sc)):
+    for coord, stride in ((a, sa), (b, sb), (c, sc_)):
         for d in (1, 2, 3):
             pl.semaphore_signal(barrier, inc=1, device_id=(ring(coord, stride, d)[1],), device_id_type=MESH)
     for d in range(1, 8):
@@ -108,28 +112,37 @@
         sends.append(copy)
         return copy
 
-    for copy in dense_in:
+    span = [pl.ds(2 * CACHE * s, 2 * CACHE) for s in range(SEQ_DEV)]
+    for copy in small_in:
         copy.wait()
-    for k, tile in enumerate((dg_ref, du_ref, dd_ref)):
-        for r in range(7):
-            wsend[r, PART * k : PART * (k + 1)] = tile[PART * r : PART * (r + 1)]
-        wsend[7, PART * k : PART * k + 16] = tile[336:352]
-        wsend[7, PART * k + 16 : PART * (k + 1)] = jnp.zeros((32, 256), bf)
-    pl.semaphore_wait(barrier, 17)
-    arrive_w = []
-    for d in range(7):
-        to, device = group(d + 1)
-        arrive_w.append(start(wsend.at[to], wrecv.at[row_block], rs_w.at[d], rr_w.at[d], device))
-    wrecv[row_block] = wsend[row_block]
-
-
     normed = rms_norm(tok_ref[...].astype(f32), again_ref[...], 1e-06).astype(bf)
     for n in range(4):
         proj_in[n].wait()
         cols = slice(256 * n, 256 * (n + 1))
+        if n == 0:
+            keys_in = [fetch(keys_hbm.at[span[s]], keys.at[s], ksem.at[s]) for s in range(SEQ_DEV)]
+        if n == 2:
+            values_in = [fetch(values_hbm.at[span[s]], values.at[s], vsem.at[s]) for s in range(SEQ_DEV)]
         qf[:, cols] = jnp.dot(normed, qw[:, cols], preferred_element_type=f32).astype(bf).astype(f32)
+        if n == 1:
+            for copy in dense_in:
+                copy.wait()
+            for k, tile in enumerate((dg_ref, du_ref, dd_ref)):
+                for r in range(7):
+                    wsend[r, PART * k : PART * (k + 1)] = tile[PART * r : PART * (r + 1)]
+                wsend[7, PART * k : PART * k + 16] = tile[336:352]
+                wsend[7, PART * k + 16 : PART * (k + 1)] = jnp.zeros((32, 256), bf)
+            pl.semaphore_wait(barrier, 17)
+            arrive_w = []
+            for d in range(7):
+                to, device = group(d + 1)
+                arrive_w.append(start(wsend.at[to], wrecv.at[row_block], rs_w.at[d], rr_w.at[d], device))
+            wrecv[row_block] = wsend[row_block]
     proj_in[4].wait()
     proj_in[5].wait()
+    out_in = [
+        fetch(ow_hbm.at[:, pl.ds(512 * n, 512)], ow.at[:, pl.ds(512 * n, 512)], osem.at[n]) for n in range(4)
+    ]
     new = jnp.dot(normed, kvw[...], preferred_element_type=f32).astype(bf)
     newk_ref[...] = new[:, :256]
     newv_ref[...] = new[:, 256:]
@@ -137,13 +150,6 @@
     for s in range(SEQ_DEV):
         for h in range(HEADS):
             qs[s, h : h + 1] = qf[s : s + 1, HEAD_DIM * h : HEAD_DIM * (h + 1)]
-
-    loads = []
-    for n in range(3):
-        cols = pl.ds(128 * n, 128)
-        loads.append(fetch(wg_hbm.at[:, cols], wgu.at[n, :, pl.ds(0, 128)], wsem.at[2 * n]))
-        loads.append(fetch(wu_hbm.at[:, cols], wgu.at[n, :, pl.ds(128, 128)], wsem.at[2 * n + 1]))
-    loads.append(fetch(wd_hbm, wdx.at[pl.ds(0, HID)], wsem.at[6]))
 
     head8 = lax.broadcasted_iota(jnp.int32, (HEADS, HEAD_DIM), 0)
     lane8 = lax.broadcasted_iota(jnp.int32, (HEADS, HEAD_DIM), 1)
@@ -166,23 +172,33 @@
 
     base = HEADS * HEAD_DIM
     for s in range(SEQ_DEV):
+        keys_in[s].wait()
+    for s in range(SEQ_DEV):
         q = qs[s]
-        q_one, q_two = jnp.where(low_lane, q, 0.0), jnp.where(low_lane, 0.0, q)
+        both = jnp.concatenate([jnp.where(low_lane, q, 0.0), jnp.where(low_lane, 0.0, q)], axis=0).astype(bf)
+        sc[s] = lax.dot_general(both, keys[s], NT, preferred_element_type=f32) * scale
+    loads = []
+    for n in range(3):
+        cols = pl.ds(128 * n, 128)
+        loads.append(fetch(wg_hbm.at[:, cols], wgu.at[n, :, pl.ds(0, 128)], wsem.at[2 * n]))
+        loads.append(fetch(wu_hbm.at[:, cols], wgu.at[n, :, pl.ds(128, 128)], wsem.at[2 * n + 1]))
+    loads.append(fetch(wd_hbm, wdx.at[pl.ds(0, HID)], wsem.at[6]))
+
+    for s in range(SEQ_DEV):
+        values_in[s].wait()
+    for s in range(SEQ_DEV):
+        q = qs[s]
         rows = [qf[s : s + 1, base + 128 * k : base + 128 * (k + 1)] for k in range(4)]
-        own_key = jnp.where(low_head, rows[0], rows[1])
+        own_score = q * jnp.where(low_head, rows[0], rows[1])
         own_value = jnp.where(low_head, rows[2], rows[3])
-        own_one = jnp.sum(q_one * own_key, axis=1, keepdims=True) * scale
-        own_two = jnp.sum(q_two * own_key, axis=1, keepdims=True) * scale
-        keys_in[s].wait()
-        both = jnp.concatenate([q_one, q_two], axis=0).astype(bf)
-        scores = lax.dot_general(both, keys[s], NT, preferred_element_type=f32) * scale
+        own_one = jnp.sum(jnp.where(low_lane, own_score, 0.0), axis=1, keepdims=True) * scale
+        own_two = jnp.sum(jnp.where(low_lane, 0.0, own_score), axis=1, keepdims=True) * scale
         valid = mine_kv & (slot < 2 * len_ref[s])
-        raised_one, own_one, inv_one = probabilities(scores[:HEADS], own_one, valid)
-        raised_two, own_two, inv_two = probabilities(scores[HEADS:], own_two, valid)
+        raised_one, own_one, inv_one = probabilities(sc[s, :HEADS], own_one, valid)
+        raised_two, own_two, inv_two = probabilities(sc[s, HEADS:], own_two, valid)
         inv_two = inv_two * lam
         weights = (raised_one * inv_one - raised_two * inv_two).astype(bf)
         own_weight = (own_one * inv_one - own_two * inv_two).astype(bf).astype(f32)
-        values_in[s].wait()
         mixed = jnp.dot(weights, values[s], preferred_element_type=f32) + own_weight * own_value
         mixed = rms_norm(mixed, hgain_ref[...], 1e-05)
         for h in range(HEADS):
@@ -230,7 +246,7 @@
         for dc in (1, 3, 2):
             arrive_c[db, dc] = start(
                 xown.at[rows16(block)], xown.at[rows16(block)],
-                cs_s.at[3 * db + dc - 1], cs_r.at[3 * db + dc - 1], ring(c, sc, dc)[1],
+                cs_s.at[3 * db + dc - 1], cs_r.at[3 * db + dc - 1], ring(c, sc_, dc)[1],
             )
         across(block)
 
@@ -280,13 +296,6 @@
         copy.wait_recv()
     hidden(xpart, 1)
 
-    arrive_2 = []
-    for n in range(CHUNKS):
-        cols = slice(COLS * n, COLS * (n + 1))
-        psend[n] = jnp.dot(act[1], wdx[:, cols], preferred_element_type=jnp.float32).astype(jnp.bfloat16)
-        arrive_2.append(start(psend.at[n], drecv.at[n], d2s.at[n], d2r.at[n], partner))
-        acc[n] = jnp.dot(act[0], wdx[:, cols], preferred_element_type=jnp.float32)
-
     def ahead(n, coord, stride, src, dst, send_sem, recv_sem, height):
         copies = []
         for d in (1, 3, 2):
@@ -300,13 +309,24 @@
             )
         return copies
 
-    arrive_c2 = []
-    for n in range(CHUNKS):
+    arrive_2, arrive_c2 = [], []
+
+    def merge(n):
         arrive_2[n].wait_recv()
         total = acc[n] + drecv[n].astype(jnp.float32)
         acc[n] = total
         csend[n] = total.astype(jnp.bfloat16)
-        arrive_c2.append(ahead(n, c, sc, csend, crecv, c2s, c2r, 64))
+        arrive_c2.append(ahead(n, c, sc_, csend, crecv, c2s, c2r, 64))
+
+    for n in range(CHUNKS):
+        cols = slice(COLS * n, COLS * (n + 1))
+        psend[n] = jnp.dot(act[1], wdx[:, cols], preferred_element_type=jnp.float32).astype(jnp.bfloat16)
+        arrive_2.append(start(psend.at[n], drecv.at[n], d2s.at[n], d2r.at[n], partner))
+        acc[n] = jnp.dot(act[0], wdx[:, cols], preferred_element_type=jnp.float32)
+        if n >= 2:
+            merge(n - 2)
+    merge(CHUNKS - 2)
+    merge(CHUNKS - 1)
     arrive_b2 = []
     for n in range(CHUNKS):
         for copy in arrive_c2[n]:
@@ -347,6 +367,15 @@
         copy.wait_send()
 
 
+def hand_over(out_in, newk_in, newv_in, out_ref, newk_ref, newv_ref, sem):
+    pairs = ((out_in, out_ref), (newk_in, newk_ref), (newv_in, newv_ref))
+    copies = [pltpu.make_async_copy(src, dst, sem.at[k]) for k, (src, dst) in enumerate(pairs)]
+    for copy in copies:
+        copy.start()
+    for copy in copies:
+        copy.wait()
+
+
 def per_device(
     tokens, lengths, cache_keys, cache_values, query_w, key_w, value_w, out_w, mix_lambda, head_gain,
     attn_gain, ffn_gain, routes, route_weights, exp_gate, exp_up, exp_down, dense_gate, dense_up,
@@ -355,19 +384,24 @@
     bf, f32 = jnp.bfloat16, jnp.float32
     dma = pltpu.SemaphoreType.DMA
     vmem = pl.BlockSpec(memory_space=pltpu.VMEM)
-    smem = pl.BlockSpec(memory_space=pltpu.SMEM)
     anywhere = pl.BlockSpec(memory_space=pl.ANY)
     kv = KV_HEADS * HEAD_DIM
-    return pl.pallas_call(
+    shapes = tuple(jax.ShapeDtypeStruct((SEQ_DEV, width), bf) for width in (D, kv, kv))
+    made = pl.pallas_call(
         layer_kernel,
-        out_shape=(
-            jax.ShapeDtypeStruct((SEQ_DEV, D), bf),
-            jax.ShapeDtypeStruct((SEQ_DEV, kv), bf),
-            jax.ShapeDtypeStruct((SEQ_DEV, kv), bf),
-        ),
-        in_specs=[smem] * 4 + [vmem] * 5 + [anywhere] * 12,
+        out_shape=tuple(pltpu.VMEM(shape.shape, bf) for shape in shapes),
+        in_specs=[anywhere] * 21,
         out_specs=(vmem, vmem, vmem),
         scratch_shapes=[
+            pltpu.SMEM((SEQ_DEV,), jnp.int32),
+            pltpu.SMEM((HEADS,), f32),
+            pltpu.SMEM((2, SEQ_DEV), jnp.int32),
+            pltpu.SMEM((2, SEQ_DEV), f32),
+            pltpu.VMEM((SEQ_DEV, D), bf),
+            pltpu.VMEM((1, D), f32),
+            pltpu.VMEM((1, D), f32),
+            pltpu.VMEM((1, HEAD_DIM), f32),
+            pltpu.VMEM((16, 128), bf),
             pltpu.VMEM((SEQ_DEV, 2 * CACHE, HEAD_DIM), bf),
             pltpu.VMEM((SEQ_DEV, 2 * CACHE, HEAD_DIM), bf),
             pltpu.VMEM((D, HEADS * HEAD_DIM), bf),
@@ -378,6 +412,7 @@
             pltpu.VMEM((352, 256), bf),
             pltpu.VMEM((SEQ_DEV, HEADS * HEAD_DIM + 2 * kv), f32),
             pltpu.VMEM((SEQ_DEV, HEADS, HEAD_DIM), f32),
+            pltpu.VMEM((SEQ_DEV, 2 * HEADS, 2 * CACHE), f32),
             pltpu.VMEM((SEQ_DEV, HEADS * HEAD_DIM), f32),
             pltpu.VMEM((SEQ_DEV, D), f32),
             pltpu.VMEM((SEQ_DEV, WIDE), bf),
@@ -402,7 +437,7 @@
             pltpu.VMEM((CHUNKS, 4, 4, COLS), f32),
             pltpu.VMEM((CHUNKS, 4, 4, COLS), bf),
             pltpu.VMEM((CHUNKS, 3, 4, COLS), bf),
-            dma((3,)), dma((6,)), dma((4,)), dma((4,)), dma((4,)),
+            dma((9,)), dma((3,)), dma((6,)), dma((4,)), dma((4,)), dma((4,)),
             dma((7,)), dma((7,)), dma((7,)), dma((3,)), dma((3,)), dma((3,)), dma((3,)),
             dma((12,)), dma((12,)), dma((16,)), dma((16,)),
             dma((CHUNKS,)), dma((CHUNKS,)),
@@ -418,6 +453,9 @@
         cache_keys.reshape(-1, HEAD_DIM), cache_values.reshape(-1, HEAD_DIM), query_w, key_w, value_w, out_w,
         exp_gate, exp_up, exp_down, dense_gate[0].T, dense_up[0].T, dense_down[0],
     )
+    return pl.pallas_call(
+        hand_over, out_shape=shapes, in_specs=[vmem] * 3, out_specs=(anywhere,) * 3, scratch_shapes=[dma((3,))]
+    )(*[pltpu.with_memory_space_constraint(piece, pltpu.VMEM) for piece in made])
 
 
 def solution(mesh):

time: 58.7 us -> 51.1 us (0.87)
  local copies, waits for them, and re-layouts: 3.81 us -> 0 us
  Pallas kernels: 54 us -> 50.3 us
    unnamed x3 -> x0, local copies, waits for them, and re-layouts: 3.81 us -> none
    pallas_call x1 -> x2, Pallas kernels: 54 us -> 50.3 us  [the longest x1 49.6 us: per_device(): pl.pallas_call(layer_kernel, out_shape=tuple((pltpu.VMEM(shape.shape, bf)...]
where the time goes in v3:
time: 51.1 us; the launch traced here: 50.9 us
  Pallas kernels  50.3 us (98%)
  between operations  0.65 us (1%)
    pallas_call x1, Pallas kernels, per_device(): pl.pallas_call(layer_kernel, out_shape=tuple((pltpu.VMEM(shape.shape, bf)...  49.6 us

profile of v3, /device:TPU:0, one launch (start us, length us, event | category | flops | bytes accessed | tf_op | source)
XLA Modules:
  0.0 50.9 jit_solution(13739386359360355631)
XLA Ops:
  0.6 49.6 %shard_map.220 = (bf16[4,2048]{1,0:T(4,128)(2,1)S(1)}, bf16[4,256]{1,0:T(4,128)(2,1)S(1)}, bf16[4,256]{1,0:T(4,128)(2,1)S(1)}) custom-call(s32[4]{0:T(128)} %len_hbm.1, f32[8]{0:T(128)} %lam_hbm.1, s32[2,4]{1,0:T(2,128)} %bitcast.23, f32[2,4]{1,0:T(2,128)} %bitcast.24, bf16[4,2048]{1,0:T(4,128)(2,1)} %tok_hbm.1, f32[1,2048]{1,0:T(1,128)} %bitcast.20, ...), custom_call_target="tpu_custom_call" | custom-call | tf_op jit(solution)/shard_map/pallas_call | solution.py:390
  50.3 0.6 %shard_map.221 = (bf16[4,2048]{1,0:T(4,128)(2,1)}, bf16[4,256]{1,0:T(4,128)(2,1)}, bf16[4,256]{1,0:T(4,128)(2,1)}) custom-call(bf16[4,2048]{1,0:T(4,128)(2,1)S(1)} %get-tuple-element.6.out_in, bf16[4,256]{1,0:T(4,128)(2,1)S(1)} %get-tuple-element.7.newk_in, bf16[4,256]{1,0:T(4,128)(2,1)S(1)} %get-tuple-element.8.newv_in), custom_call_target="tpu_custom_call" | custom-call | tf_op jit(solution)/shard_map/pallas_call | solution.py:456

commit v4 on v3

v4 whole, which is shorter than its diff:
```python
import jax
import jax.numpy as jnp
from jax import lax
from jax.experimental import pallas as pl
from jax.experimental.pallas import tpu as pltpu
from jax.sharding import PartitionSpec as P

HEADS = 8
KV_HEADS = 2
HEAD_DIM = 128
SEQ_DEV = 4
CACHE = 1024
SPLIT = 16
D = 2048
SIDE = 128
WIDE = D + SIDE
HID = 384
PART = 48
CHUNKS = 4
EDGE = 5 * 128
VMEM_LIMIT = 67043328 - 131072
COLS = D // CHUNKS
MESH = pl.DeviceIdType.MESH
NT = (((1,), (1,)), ((), ()))


def rms_norm(values, gain, epsilon):
    scale = lax.rsqrt(jnp.mean(values * values, axis=-1, keepdims=True) + epsilon)
    return values * scale * gain


def remote(src, dst, send, recv, device):
    return pltpu.make_async_remote_copy(
        src_ref=src, dst_ref=dst, send_sem=send, recv_sem=recv,
        device_id=(device,), device_id_type=MESH,
    )


def layer_kernel(
    len_hbm, lam_hbm, routes_hbm, rweights_hbm, tok_hbm, again_hbm, fgain_hbm, hgain_hbm, bgate_hbm,
    keys_hbm, values_hbm, qw_hbm, kw_hbm, vw_hbm, ow_hbm,
    wg_hbm, wu_hbm, wd_hbm, dg_hbm, du_hbm, dd_hbm,
    out_ref, newk_ref, newv_ref,
    len_ref, lam_ref, routes_ref, rweights_ref, tok_ref, again_ref, fgain_ref, hgain_ref, bgate_ref,
    keys, values, qw, kvw, ow, tiles, qf, qs, sc, hf, hid_ref, x_ref,
    wgu, wdx, wsend, wrecv, land0, land1, pack, xown, xpart, act, acc, psend, drecv, csend, crecv,
    bsum, aown, asend, arecv,
    isem, dsem, qsem, ksem, vsem, osem,
    wsem, rs_w, rr_w, as_s, as_r, cs_s, cs_r, ds_s, ds_r, d2s, d2r, c2s, c2r, a2s, a2r,
):
    me = lax.axis_index("ep")
    core = lax.rem(me, 2)
    x = lax.rem(lax.div(me, 2), 4)
    y = lax.rem(lax.div(me, 8), 4)
    z = lax.div(me, 32)
    other = 1 - core
    a, sa = x * other + y * core, 2 * other + 8 * core
    p, sp = y * other + x * core, 8 * other + 2 * core
    colours = ((p, sp, z, 32), (z, 32, p, sp))
    row_block = lax.div(me, SPLIT)
    partner = me + other - core

    def ring(coord, stride, d):
        new = lax.rem(coord + d, 4)
        return new, me + (new - coord) * stride

    def plane(coord, stride, db, da):
        new_b, new_a = lax.rem(coord + db, 4), lax.rem(a + da, 4)
        return new_b, new_a, me + (new_b - coord) * stride + (new_a - a) * sa

    def group(d):
        new = lax.rem(row_block + d, 8)
        return new, me + (new - row_block) * SPLIT

    bf, f32 = jnp.bfloat16, jnp.float32

    def fetch(src, dst, sem):
        copy = pltpu.make_async_copy(src, dst, sem)
        copy.start()
        return copy

    for k, tile in enumerate((dg_hbm, du_hbm, dd_hbm)):
        fetch(tile, tiles.at[k], dsem)
    small = (
        (tok_hbm, tok_ref), (again_hbm, again_ref), (len_hbm, len_ref), (lam_hbm, lam_ref),
        (routes_hbm, routes_ref), (rweights_hbm, rweights_ref), (fgain_hbm, fgain_ref),
        (hgain_hbm, hgain_ref), (bgate_hbm, bgate_ref),
    )
    small_in = [fetch(src, dst, isem.at[k]) for k, (src, dst) in enumerate(small)]
    quarter = [pl.ds(256 * n, 256) for n in range(4)]
    proj_in = [fetch(qw_hbm.at[:, part], qw.at[:, part], qsem.at[k]) for k, part in enumerate(quarter[:2])]
    barrier = pltpu.get_barrier_semaphore()
    for coord, stride, _, _ in colours:
        for k in range(1, 16):
            device = plane(coord, stride, k // 4, k % 4)[2]
            pl.semaphore_signal(barrier, inc=1, device_id=(device,), device_id_type=MESH)
    for d in range(1, 8):
        pl.semaphore_signal(barrier, inc=1, device_id=(group(d)[1],), device_id_type=MESH)
    pl.semaphore_signal(barrier, inc=1, device_id=(partner,), device_id_type=MESH)

    def start(*args):
        remote(*args).start()

    for copy in small_in:
        copy.wait()
    proj_in += [fetch(qw_hbm.at[:, part], qw.at[:, part], qsem.at[2 + k]) for k, part in enumerate(quarter[2:])]
    fetch(kw_hbm, kvw.at[:, pl.ds(0, 256)], qsem.at[4])
    fetch(vw_hbm, kvw.at[:, pl.ds(256, 256)], qsem.at[4])
    landed(tiles, dsem)
    for k in range(3):
        for r in range(7):
            wsend[r, PART * k : PART * (k + 1)] = tiles[k, PART * r : PART * (r + 1)]
        wsend[7, PART * k : PART * k + 16] = tiles[k, 336:352]
        wsend[7, PART * k + 16 : PART * (k + 1)] = jnp.zeros((32, 256), bf)
    pl.semaphore_wait(barrier, 38)
    for d in range(1, 8):
        to, device = group(d)
        start(wsend.at[to], wrecv.at[row_block], rs_w, rr_w, device)
    wrecv[row_block] = wsend[row_block]
    normed = rms_norm(tok_ref[...].astype(f32), again_ref[...], 1e-06).astype(bf)
    for n in range(4):
        proj_in[n].wait()
        cols = slice(256 * n, 256 * (n + 1))
        if n == 0:
            fetch(keys_hbm, keys, ksem)
        if n == 2:
            fetch(values_hbm, values, vsem)
        qf[:, cols] = jnp.dot(normed, qw[:, cols], preferred_element_type=f32).astype(bf).astype(f32)
    landed(kvw, qsem.at[4])
    out_in = [
        fetch(ow_hbm.at[:, pl.ds(512 * n, 512)], ow.at[:, pl.ds(512 * n, 512)], osem.at[n]) for n in range(4)
    ]
    new = jnp.dot(normed, kvw[...], preferred_element_type=f32).astype(bf)
    newk_ref[...] = new[:, :256]
    newv_ref[...] = new[:, 256:]
    qf[:, HEADS * HEAD_DIM :] = new.astype(f32)
    for s in range(SEQ_DEV):
        for h in range(HEADS):
            qs[s, h : h + 1] = qf[s : s + 1, HEAD_DIM * h : HEAD_DIM * (h + 1)]

    head8 = lax.broadcasted_iota(jnp.int32, (HEADS, HEAD_DIM), 0)
    lane8 = lax.broadcasted_iota(jnp.int32, (HEADS, HEAD_DIM), 1)
    low_head, low_lane = head8 < HEADS // KV_HEADS, lane8 < HEAD_DIM // 2
    head1 = lax.broadcasted_iota(jnp.int32, (HEADS, 1), 0)
    lam = jnp.zeros((HEADS, 1), f32)
    for h in range(HEADS):
        lam = jnp.where(head1 == h, lam_ref[h], lam)
    slot = lax.broadcasted_iota(jnp.int32, (HEADS, 2 * CACHE), 1)
    kv_of = lax.broadcasted_iota(jnp.int32, (HEADS, 2 * CACHE), 0) // (HEADS // KV_HEADS)
    mine_kv = (slot & 1) == kv_of
    scale = (HEAD_DIM // 2) ** (-0.5)

    def probabilities(scores, own, valid):
        largest = jnp.maximum(jnp.max(jnp.where(valid, scores, -jnp.inf), axis=1, keepdims=True), own)
        raised = jnp.where(valid, jnp.exp(scores - largest), 0.0)
        own_raised = jnp.exp(own - largest)
        total = jnp.sum(raised, axis=1, keepdims=True) + own_raised
        return raised, own_raised, 1.0 / total

    base = HEADS * HEAD_DIM
    landed(keys, ksem)
    for s in range(SEQ_DEV):
        q = qs[s]
        both = jnp.concatenate([jnp.where(low_lane, q, 0.0), jnp.where(low_lane, 0.0, q)], axis=0).astype(bf)
        sc[s] = lax.dot_general(both, keys[s], NT, preferred_element_type=f32) * scale
    for n in range(3):
        cols = pl.ds(128 * n, 128)
        fetch(wg_hbm.at[:, cols], wgu.at[n, :, pl.ds(0, 128)], wsem.at[0])
        fetch(wu_hbm.at[:, cols], wgu.at[n, :, pl.ds(128, 128)], wsem.at[0])
    fetch(wd_hbm, wdx.at[pl.ds(0, HID)], wsem.at[1])
    landed(values, vsem)
    for s in range(SEQ_DEV):
        q = qs[s]
        rows = [qf[s : s + 1, base + 128 * k : base + 128 * (k + 1)] for k in range(4)]
        own_score = q * jnp.where(low_head, rows[0], rows[1])
        own_value = jnp.where(low_head, rows[2], rows[3])
        own_one = jnp.sum(jnp.where(low_lane, own_score, 0.0), axis=1, keepdims=True) * scale
        own_two = jnp.sum(jnp.where(low_lane, 0.0, own_score), axis=1, keepdims=True) * scale
        valid = mine_kv & (slot < 2 * len_ref[s])
        raised_one, own_one, inv_one = probabilities(sc[s, :HEADS], own_one, valid)
        raised_two, own_two, inv_two = probabilities(sc[s, HEADS:], own_two, valid)
        inv_two = inv_two * lam
        weights = (raised_one * inv_one - raised_two * inv_two).astype(bf)
        own_weight = (own_one * inv_one - own_two * inv_two).astype(bf).astype(f32)
        mixed = jnp.dot(weights, values[s], preferred_element_type=f32) + own_weight * own_value
        mixed = rms_norm(mixed, hgain_ref[...], 1e-05)
        for h in range(HEADS):
            hf[s : s + 1, HEAD_DIM * h : HEAD_DIM * (h + 1)] = mixed[h : h + 1]
    heads = hf[...].astype(bf)
    for n in range(4):
        out_in[n].wait()
        cols = slice(512 * n, 512 * (n + 1))
        hid_ref[:, cols] = tok_ref[:, cols].astype(f32) + jnp.dot(heads, ow[:, cols], preferred_element_type=f32)
    ffn_in = rms_norm(hid_ref[...], fgain_ref[...], 1e-06).astype(bf)
    gate_row = bgate_ref[...].astype(f32)
    terms = jnp.zeros((SEQ_DEV, 128), f32)
    for k in range(16):
        terms = terms + ffn_in[:, 128 * k : 128 * (k + 1)].astype(f32) * gate_row[k : k + 1]
    gate = jax.nn.sigmoid(jnp.sum(terms, axis=1, keepdims=True))
    place = lax.broadcasted_iota(jnp.int32, (SEQ_DEV, SIDE), 1)
    row = lax.broadcasted_iota(jnp.int32, (SEQ_DEV, SIDE), 0)
    full = jnp.where((place == 16) | (place == 17), gate, 0.0)
    for t in range(SEQ_DEV):
        for k in range(2):
            chosen = (row == t) & (place < 16) & ((place & 7) == routes_ref[k, t])
            full = full + jnp.where(chosen, rweights_ref[k, t], 0.0)
    high = full.astype(bf).astype(f32)
    side = jnp.where((place < 8) | (place == 16), high, full - high)
    x_ref[:, :D] = ffn_in
    x_ref[:, D:] = side.astype(bf)

    lanes = (slice(0, EDGE), slice(EDGE, WIDE))
    spans = (pl.ds(0, EDGE), pl.ds(EDGE, WIDE - EDGE))
    lands = (land0, land1)
    for k in (1, 2, 3, 4, 5, 6, 7, 12, 13, 14, 15, 8, 9, 10, 11):
        for s, (coord, stride, _, _) in enumerate(colours):
            device = plane(coord, stride, k // 4, k % 4)[2]
            start(x_ref.at[:, spans[s]], lands[s].at[4 * coord + a], as_s.at[s], as_r.at[s, k // 4], device)
    for s, (coord, _, _, _) in enumerate(colours):
        lands[s][4 * coord + a] = x_ref[:, lanes[s]]

    def place_of(s, along_c, along_b):
        return (along_c, along_b) if s == 0 else (along_b, along_c)

    def across(s, place):
        at = (*place, slice(None), spans[s])
        start(xown.at[at], xpart.at[at], ds_s, ds_r, partner)

    order = (0, 1, 3, 2)
    for db in order:
        for s, (b, _, c, sc_) in enumerate(colours):
            landed(lands[s].at[pl.ds(0, 4 if db else 3)], as_r.at[s, db])
            row = lax.rem(b + 4 - db, 4)
            for j in range(4):
                pack[4 * j : 4 * j + 4, lanes[s]] = lands[s][4 * row + j].astype(f32)
            place = place_of(s, c, row)
            xown[(*place, slice(None), lanes[s])] = pack[:, lanes[s]].astype(bf)
            at = (*place, slice(None), spans[s])
            for dc in (1, 3, 2):
                start(xown.at[at], xown.at[at], cs_s.at[s], cs_r.at[s, db], ring(c, sc_, dc)[1])
            across(s, place)
    for db in order:
        for s, (b, _, c, _) in enumerate(colours):
            landed(xown.at[0, pl.ds(0, 3), :, spans[s]], cs_r.at[s, db])
            for dc in (1, 3, 2):
                across(s, place_of(s, lax.rem(c + 4 - dc, 4), lax.rem(b + 4 - db, 4)))

    landed(wgu, wsem.at[0])
    landed(wdx.at[pl.ds(0, HID)], wsem.at[1])
    landed(wrecv.at[pl.ds(0, 7)], rr_w)
    wdx[HID + PART :] = jnp.zeros((128 - PART, D), jnp.bfloat16)
    for r in range(8):
        wdx[HID : HID + PART, 256 * r : 256 * (r + 1)] = wrecv[r, 2 * PART :]

    lane = lax.broadcasted_iota(jnp.int32, (256, SIDE), 1)

    def hidden(rows, k):
        side = rows[:, D:].astype(jnp.float32)
        expert = lax.div(me, SPLIT)
        weight = jnp.sum(jnp.where((lane == expert) | (lane == expert + 8), side, 0.0), axis=1, keepdims=True)
        gate = jnp.sum(jnp.where((lane == 16) | (lane == 17), side, 0.0), axis=1, keepdims=True)
        for n in range(3):
            both = jnp.dot(rows[:, :D], wgu[n], preferred_element_type=jnp.float32)
            first, second = both[:, :128], both[:, 128:]
            act[k, :, 128 * n : 128 * (n + 1)] = (first * jax.nn.sigmoid(first) * second * weight).astype(jnp.bfloat16)
        both = jnp.zeros((256, 128), jnp.float32)
        for r in range(8):
            both += lax.dot_general(
                rows[:, 256 * r : 256 * (r + 1)], wrecv[r, 0:128], NT, preferred_element_type=jnp.float32
            )
        second = pltpu.roll(both, 128 - PART, 1)
        value = both * jax.nn.sigmoid(both) * second * gate
        act[k, :, HID:] = jnp.where(lane < PART, value, 0.0).astype(jnp.bfloat16)

    def merge(n):
        landed(drecv.at[n], d2r.at[n])
        total = acc[n] + drecv[n].astype(f32)
        acc[n] = total
        csend[n] = total.astype(bf)
        s = min(n, 1)
        c, sc_ = colours[s][2:]
        for d in (1, 3, 2):
            to, device = ring(c, sc_, d)
            start(csend.at[n, to] if s == 0 else csend.at[n, :, to], crecv.at[n, d - 1], c2s, c2r.at[n], device)

    hidden(xown[...].reshape(256, WIDE), 0)
    landed(xpart, ds_r)
    hidden(xpart[...].reshape(256, WIDE), 1)
    for n in range(CHUNKS):
        cols = slice(COLS * n, COLS * (n + 1))
        psend[n] = jnp.dot(act[1], wdx[:, cols], preferred_element_type=f32).astype(bf).reshape(4, 4, 16, COLS)
        start(psend.at[n], drecv.at[n], d2s, d2r.at[n], partner)
    for n in range(CHUNKS):
        cols = slice(COLS * n, COLS * (n + 1))
        acc[n] = jnp.dot(act[0], wdx[:, cols], preferred_element_type=f32).reshape(4, 4, 16, COLS)
        merge(n)
    for n in range(CHUNKS):
        s = min(n, 1)
        b, sb, c, _ = colours[s]
        landed(crecv.at[n], c2r.at[n])
        total = acc[n, c] if s == 0 else acc[n, :, c]
        for d in range(3):
            total = total + crecv[n, d].astype(f32)
        bsum[n] = total
        for k in range(4):
            for j in range(4):
                piece = bsum[n, k, 4 * j : 4 * j + 4]
                aown[n, k, j] = piece
                asend[n, k, j] = piece.astype(bf)
        for k in (1, 2, 3, 4, 5, 6, 7, 12, 13, 14, 15, 8, 9, 10, 11):
            to_b, to_a, device = plane(b, sb, k // 4, k % 4)
            start(asend.at[n, to_b, to_a], arecv.at[n, k - 1], a2s, a2r.at[n], device)
    for n in range(CHUNKS):
        cols = slice(COLS * n, COLS * (n + 1))
        total = hid_ref[:, cols] + aown[n, colours[min(n, 1)][0], a]
        landed(arecv.at[n], a2r.at[n])
        for k in range(15):
            total = total + arecv[n, k].astype(f32)
        out_ref[:, cols] = total.astype(bf)
    landed(wsend.at[pl.ds(0, 7)], rs_w)
    for s in range(2):
        landed(lands[s].at[pl.ds(0, 15)], as_s.at[s])
        landed(xown.at[pl.ds(0, 3), :, :, spans[s]], cs_s.at[s])
    landed(xown, ds_s)
    landed(psend, d2s)
    landed(crecv, c2s)
    landed(arecv, a2s)


def landed(ref, sem):
    pltpu.make_async_copy(ref, ref, sem).wait()


def hand_over(out_in, newk_in, newv_in, out_ref, newk_ref, newv_ref, sem):
    pairs = ((out_in, out_ref), (newk_in, newk_ref), (newv_in, newv_ref))
    copies = [pltpu.make_async_copy(src, dst, sem.at[k]) for k, (src, dst) in enumerate(pairs)]
    for copy in copies:
        copy.start()
    for copy in copies:
        copy.wait()


def per_device(
    tokens, lengths, cache_keys, cache_values, query_w, key_w, value_w, out_w, mix_lambda, head_gain,
    attn_gain, ffn_gain, routes, route_weights, exp_gate, exp_up, exp_down, dense_gate, dense_up,
    dense_down, branch_gate,
):
    bf, f32 = jnp.bfloat16, jnp.float32
    dma = pltpu.SemaphoreType.DMA
    vmem = pl.BlockSpec(memory_space=pltpu.VMEM)
    anywhere = pl.BlockSpec(memory_space=pl.ANY)
    kv = KV_HEADS * HEAD_DIM
    shapes = tuple(jax.ShapeDtypeStruct((SEQ_DEV, width), bf) for width in (D, kv, kv))
    made = pl.pallas_call(
        layer_kernel,
        out_shape=tuple(pltpu.VMEM(shape.shape, bf) for shape in shapes),
        in_specs=[anywhere] * 21,
        out_specs=(vmem, vmem, vmem),
        scratch_shapes=[
            pltpu.SMEM((SEQ_DEV,), jnp.int32),
            pltpu.SMEM((HEADS,), f32),
            pltpu.SMEM((2, SEQ_DEV), jnp.int32),
            pltpu.SMEM((2, SEQ_DEV), f32),
            pltpu.VMEM((SEQ_DEV, D), bf),
            pltpu.VMEM((1, D), f32),
            pltpu.VMEM((1, D), f32),
            pltpu.VMEM((1, HEAD_DIM), f32),
            pltpu.VMEM((16, 128), bf),
            pltpu.VMEM((SEQ_DEV, 2 * CACHE, HEAD_DIM), bf),
            pltpu.VMEM((SEQ_DEV, 2 * CACHE, HEAD_DIM), bf),
            pltpu.VMEM((D, HEADS * HEAD_DIM), bf),
            pltpu.VMEM((D, 2 * kv), bf),
            pltpu.VMEM((HEADS * HEAD_DIM, D), bf),
            pltpu.VMEM((3, 352, 256), bf),
            pltpu.VMEM((SEQ_DEV, HEADS * HEAD_DIM + 2 * kv), f32),
            pltpu.VMEM((SEQ_DEV, HEADS, HEAD_DIM), f32),
            pltpu.VMEM((SEQ_DEV, 2 * HEADS, 2 * CACHE), f32),
            pltpu.VMEM((SEQ_DEV, HEADS * HEAD_DIM), f32),
            pltpu.VMEM((SEQ_DEV, D), f32),
            pltpu.VMEM((SEQ_DEV, WIDE), bf),
            pltpu.VMEM((3, D, 256), bf),
            pltpu.VMEM((512, D), bf),
            pltpu.VMEM((8, 3 * PART, 256), bf),
            pltpu.VMEM((8, 3 * PART, 256), bf),
            pltpu.VMEM((16, SEQ_DEV, EDGE), bf),
            pltpu.VMEM((16, SEQ_DEV, WIDE - EDGE), bf),
            pltpu.VMEM((16, WIDE), f32),
            pltpu.VMEM((4, 4, 16, WIDE), bf),
            pltpu.VMEM((4, 4, 16, WIDE), bf),
            pltpu.VMEM((2, 256, 512), bf),
            pltpu.VMEM((CHUNKS, 4, 4, 16, COLS), f32),
            pltpu.VMEM((CHUNKS, 4, 4, 16, COLS), bf),
            pltpu.VMEM((CHUNKS, 4, 4, 16, COLS), bf),
            pltpu.VMEM((CHUNKS, 4, 4, 16, COLS), bf),
            pltpu.VMEM((CHUNKS, 3, 4, 16, COLS), bf),
            pltpu.VMEM((CHUNKS, 4, 16, COLS), f32),
            pltpu.VMEM((CHUNKS, 4, 4, SEQ_DEV, COLS), f32),
            pltpu.VMEM((CHUNKS, 4, 4, SEQ_DEV, COLS), bf),
            pltpu.VMEM((CHUNKS, 15, SEQ_DEV, COLS), bf),
            dma((9,)), dma, dma((5,)), dma, dma, dma((4,)),
            dma((2,)), dma, dma, dma((2,)), dma((2, 4)), dma((2,)), dma((2, 4)), dma, dma,
            dma, dma((CHUNKS,)), dma, dma((CHUNKS,)), dma, dma((CHUNKS,)),
        ],
        compiler_params=pltpu.CompilerParams(
            collective_id=0, has_side_effects=True, vmem_limit_bytes=VMEM_LIMIT
        ),
    )(
        lengths, mix_lambda, routes.T, route_weights.T, tokens, attn_gain.reshape(1, D), ffn_gain.reshape(1, D), head_gain.reshape(1, HEAD_DIM),
        branch_gate.reshape(16, 128),
        cache_keys.reshape(SEQ_DEV, -1, HEAD_DIM), cache_values.reshape(SEQ_DEV, -1, HEAD_DIM), query_w, key_w, value_w, out_w,
        exp_gate, exp_up, exp_down, dense_gate[0].T, dense_up[0].T, dense_down[0],
    )
    return pl.pallas_call(
        hand_over, out_shape=shapes, in_specs=[vmem] * 3, out_specs=(anywhere,) * 3, scratch_shapes=[dma((3,))]
    )(*[pltpu.with_memory_space_constraint(piece, pltpu.VMEM) for piece in made])


def solution(mesh):
    placed = (
        P("ep", None), P("ep"), P("ep", None, None, None), P("ep", None, None, None),
        P(), P(), P(), P(), P(), P(), P(), P(),
        P("ep", None), P("ep", None), P(None, "ep"), P(None, "ep"), P("ep", None),
        P("ep", None, None), P("ep", None, None), P("ep", None, None), P(),
    )
    return jax.shard_map(
        per_device,
        mesh=mesh,
        in_specs=placed,
        out_specs=(P("ep", None), P("ep", None), P("ep", None)),
        check_vma=False,
    )
```

time: 51.1 us -> 43.3 us (0.85)
  Pallas kernels: 50.3 us -> 42.5 us
    pallas_call x1, Pallas kernels: 49.6 us -> 41.8 us  [per_device(): pl.pallas_call(layer_kernel, out_shape=tuple((pltpu.VMEM(shape.shape, bf)...]
where the time goes in v4:
time: 43.3 us; the launch traced here: 43.1 us
  Pallas kernels  42.5 us (98%)
  between operations  0.65 us (2%)
    pallas_call x1, Pallas kernels, per_device(): pl.pallas_call(layer_kernel, out_shape=tuple((pltpu.VMEM(shape.shape, bf)...  41.8 us

profile of v4, /device:TPU:0, one launch (start us, length us, event | category | flops | bytes accessed | tf_op | source)
XLA Modules:
  0.0 43.1 jit_solution(15625963730970273677)
XLA Ops:
  0.6 41.8 %shard_map.220 = (bf16[4,2048]{1,0:T(4,128)(2,1)S(1)}, bf16[4,256]{1,0:T(4,128)(2,1)S(1)}, bf16[4,256]{1,0:T(4,128)(2,1)S(1)}) custom-call(s32[4]{0:T(128)} %len_hbm.1, f32[8]{0:T(128)} %lam_hbm.1, s32[2,4]{1,0:T(2,128)} %bitcast.23, f32[2,4]{1,0:T(2,128)} %bitcast.24, bf16[4,2048]{1,0:T(4,128)(2,1)} %tok_hbm.1, f32[1,2048]{1,0:T(1,128)} %bitcast.20, ...), custom_call_target="tpu_custom_call" | custom-call | tf_op jit(solution)/shard_map/pallas_call | solution.py:354
  42.5 0.6 %shard_map.221 = (bf16[4,2048]{1,0:T(4,128)(2,1)}, bf16[4,256]{1,0:T(4,128)(2,1)}, bf16[4,256]{1,0:T(4,128)(2,1)}) custom-call(bf16[4,2048]{1,0:T(4,128)(2,1)S(1)} %get-tuple-element.6.out_in, bf16[4,256]{1,0:T(4,128)(2,1)S(1)} %get-tuple-element.7.newk_in, bf16[4,256]{1,0:T(4,128)(2,1)S(1)} %get-tuple-element.8.newv_in), custom_call_target="tpu_custom_call" | custom-call | tf_op jit(solution)/shard_map/pallas_call | solution.py:413

commit v5 on v4

--- a/solution.py
+++ b/solution.py
@@ -16,11 +16,13 @@
 WIDE = D + SIDE
 HID = 384
 PART = 48
-CHUNKS = 4
-EDGE = 5 * 128
+CHUNKS = ((0, 512, 1), (512, 512, 1), (1024, 640, 0), (1664, 384, 1))
+HALVES = ((0, 1024, (0, 1)), (1024, 1024, (2, 3)))
+EDGE = 6 * 128
 VMEM_LIMIT = 67043328 - 131072
-COLS = D // CHUNKS
 MESH = pl.DeviceIdType.MESH
+FAR_FIRST = (10, 6, 14, 9, 11, 2, 8, 5, 7, 13, 15, 1, 3, 4, 12)
+NEAR_FIRST = (1, 2, 3, 4, 5, 6, 7, 12, 13, 14, 15, 8, 9, 10, 11)
 NT = (((1,), (1,)), ((), ()))
 
 
@@ -74,9 +76,9 @@
 
     bf, f32 = jnp.bfloat16, jnp.float32
 
-    def fetch(src, dst, sem):
+    def fetch(src, dst, sem, priority=0):
         copy = pltpu.make_async_copy(src, dst, sem)
-        copy.start()
+        copy.start(priority=priority)
         return copy
 
     for k, tile in enumerate((dg_hbm, du_hbm, dd_hbm)):
@@ -88,7 +90,9 @@
     )
     small_in = [fetch(src, dst, isem.at[k]) for k, (src, dst) in enumerate(small)]
     quarter = [pl.ds(256 * n, 256) for n in range(4)]
-    proj_in = [fetch(qw_hbm.at[:, part], qw.at[:, part], qsem.at[k]) for k, part in enumerate(quarter[:2])]
+    proj_in = [fetch(qw_hbm.at[:, part], qw.at[:, part], qsem.at[k], 1) for k, part in enumerate(quarter)]
+    fetch(kw_hbm, kvw.at[:, pl.ds(0, 256)], qsem.at[4], 1)
+    fetch(vw_hbm, kvw.at[:, pl.ds(256, 256)], qsem.at[4], 1)
     barrier = pltpu.get_barrier_semaphore()
     for coord, stride, _, _ in colours:
         for k in range(1, 16):
@@ -103,9 +107,6 @@
 
     for copy in small_in:
         copy.wait()
-    proj_in += [fetch(qw_hbm.at[:, part], qw.at[:, part], qsem.at[2 + k]) for k, part in enumerate(quarter[2:])]
-    fetch(kw_hbm, kvw.at[:, pl.ds(0, 256)], qsem.at[4])
-    fetch(vw_hbm, kvw.at[:, pl.ds(256, 256)], qsem.at[4])
     landed(tiles, dsem)
     for k in range(3):
         for r in range(7):
@@ -122,9 +123,9 @@
         proj_in[n].wait()
         cols = slice(256 * n, 256 * (n + 1))
         if n == 0:
-            fetch(keys_hbm, keys, ksem)
+            fetch(keys_hbm, keys, ksem, 1)
         if n == 2:
-            fetch(values_hbm, values, vsem)
+            fetch(values_hbm, values, vsem, 1)
         qf[:, cols] = jnp.dot(normed, qw[:, cols], preferred_element_type=f32).astype(bf).astype(f32)
     landed(kvw, qsem.at[4])
     out_in = [
@@ -212,7 +213,7 @@
     lanes = (slice(0, EDGE), slice(EDGE, WIDE))
     spans = (pl.ds(0, EDGE), pl.ds(EDGE, WIDE - EDGE))
     lands = (land0, land1)
-    for k in (1, 2, 3, 4, 5, 6, 7, 12, 13, 14, 15, 8, 9, 10, 11):
+    for k in NEAR_FIRST:
         for s, (coord, stride, _, _) in enumerate(colours):
             device = plane(coord, stride, k // 4, k % 4)[2]
             start(x_ref.at[:, spans[s]], lands[s].at[4 * coord + a], as_s.at[s], as_r.at[s, k // 4], device)
@@ -254,68 +255,79 @@
 
     lane = lax.broadcasted_iota(jnp.int32, (256, SIDE), 1)
 
-    def hidden(rows, k):
-        side = rows[:, D:].astype(jnp.float32)
-        expert = lax.div(me, SPLIT)
-        weight = jnp.sum(jnp.where((lane == expert) | (lane == expert + 8), side, 0.0), axis=1, keepdims=True)
-        gate = jnp.sum(jnp.where((lane == 16) | (lane == 17), side, 0.0), axis=1, keepdims=True)
-        for n in range(3):
-            both = jnp.dot(rows[:, :D], wgu[n], preferred_element_type=jnp.float32)
-            first, second = both[:, :128], both[:, 128:]
-            act[k, :, 128 * n : 128 * (n + 1)] = (first * jax.nn.sigmoid(first) * second * weight).astype(jnp.bfloat16)
-        both = jnp.zeros((256, 128), jnp.float32)
-        for r in range(8):
-            both += lax.dot_general(
-                rows[:, 256 * r : 256 * (r + 1)], wrecv[r, 0:128], NT, preferred_element_type=jnp.float32
-            )
-        second = pltpu.roll(both, 128 - PART, 1)
-        value = both * jax.nn.sigmoid(both) * second * gate
-        act[k, :, HID:] = jnp.where(lane < PART, value, 0.0).astype(jnp.bfloat16)
+    def hidden(source, k, parts):
+        rows = source[...].reshape(256, WIDE)
+        side = rows[:, D:].astype(f32)
+        for n in parts:
+            if n < 3:
+                expert = lax.div(me, SPLIT)
+                weight = jnp.sum(jnp.where((lane == expert) | (lane == expert + 8), side, 0.0), axis=1, keepdims=True)
+                both = jnp.dot(rows[:, :D], wgu[n], preferred_element_type=f32)
+                first, second = both[:, :128], both[:, 128:]
+                value = first * jax.nn.sigmoid(first) * second * weight
+            else:
+                gate = jnp.sum(jnp.where((lane == 16) | (lane == 17), side, 0.0), axis=1, keepdims=True)
+                both = jnp.zeros((256, 128), f32)
+                for r in range(8):
+                    both += lax.dot_general(
+                        rows[:, 256 * r : 256 * (r + 1)], wrecv[r, 0:128], NT, preferred_element_type=f32
+                    )
+                second = pltpu.roll(both, 128 - PART, 1)
+                value = jnp.where(lane < PART, both * jax.nn.sigmoid(both) * second * gate, 0.0)
+            act[k, :, 128 * n : 128 * (n + 1)] = value.astype(bf)
 
     def merge(n):
-        landed(drecv.at[n], d2r.at[n])
-        total = acc[n] + drecv[n].astype(f32)
-        acc[n] = total
-        csend[n] = total.astype(bf)
-        s = min(n, 1)
+        low, width, s = CHUNKS[n]
+        cols, span = slice(low, low + width), pl.ds(low, width)
+        landed(drecv.at[:, :, :, span], d2r.at[n])
+        total = acc[:, :, :, cols] + drecv[:, :, :, cols].astype(f32)
+        acc[:, :, :, cols] = total
+        csend[:, :, :, cols] = total.astype(bf)
         c, sc_ = colours[s][2:]
-        for d in (1, 3, 2):
+        for d in (2, 1, 3):
             to, device = ring(c, sc_, d)
-            start(csend.at[n, to] if s == 0 else csend.at[n, :, to], crecv.at[n, d - 1], c2s, c2r.at[n], device)
-
-    hidden(xown[...].reshape(256, WIDE), 0)
+            src = csend.at[to, :, :, span] if s == 0 else csend.at[:, to, :, span]
+            start(src, crecv.at[d - 1, :, :, span], c2s, c2r.at[n], device)
+
+    hidden(xown, 0, (0, 1))
     landed(xpart, ds_r)
-    hidden(xpart[...].reshape(256, WIDE), 1)
-    for n in range(CHUNKS):
-        cols = slice(COLS * n, COLS * (n + 1))
-        psend[n] = jnp.dot(act[1], wdx[:, cols], preferred_element_type=f32).astype(bf).reshape(4, 4, 16, COLS)
-        start(psend.at[n], drecv.at[n], d2s, d2r.at[n], partner)
-    for n in range(CHUNKS):
-        cols = slice(COLS * n, COLS * (n + 1))
-        acc[n] = jnp.dot(act[0], wdx[:, cols], preferred_element_type=f32).reshape(4, 4, 16, COLS)
-        merge(n)
-    for n in range(CHUNKS):
-        s = min(n, 1)
+    hidden(xpart, 1, (0, 1, 2, 3))
+    for low, width, chunks in HALVES:
+        cols = slice(low, low + width)
+        part = jnp.dot(act[1], wdx[:, cols], preferred_element_type=f32).astype(bf)
+        psend[:, :, :, cols] = part.reshape(4, 4, 16, width)
+        for n in chunks:
+            span = pl.ds(*CHUNKS[n][:2])
+            start(psend.at[:, :, :, span], drecv.at[:, :, :, span], d2s, d2r.at[n], partner)
+    hidden(xown, 0, (2, 3))
+    for low, width, chunks in HALVES:
+        cols = slice(low, low + width)
+        part = jnp.dot(act[0], wdx[:, cols], preferred_element_type=f32)
+        acc[:, :, :, cols] = part.reshape(4, 4, 16, width)
+        for n in chunks:
+            merge(n)
+    for n, (low, width, s) in enumerate(CHUNKS):
+        cols, span = slice(low, low + width), pl.ds(low, width)
         b, sb, c, _ = colours[s]
-        landed(crecv.at[n], c2r.at[n])
-        total = acc[n, c] if s == 0 else acc[n, :, c]
+        landed(crecv.at[:, :, :, span], c2r.at[n])
+        total = acc[c, :, :, cols] if s == 0 else acc[:, c, :, cols]
         for d in range(3):
-            total = total + crecv[n, d].astype(f32)
-        bsum[n] = total
+            total = total + crecv[d, :, :, cols].astype(f32)
+        bsum[:, :, cols] = total
         for k in range(4):
             for j in range(4):
-                piece = bsum[n, k, 4 * j : 4 * j + 4]
-                aown[n, k, j] = piece
-                asend[n, k, j] = piece.astype(bf)
-        for k in (1, 2, 3, 4, 5, 6, 7, 12, 13, 14, 15, 8, 9, 10, 11):
+                piece = bsum[k, 4 * j : 4 * j + 4, cols]
+                aown[k, j, :, cols] = piece
+                asend[k, j, :, cols] = piece.astype(bf)
+        for k in FAR_FIRST:
             to_b, to_a, device = plane(b, sb, k // 4, k % 4)
-            start(asend.at[n, to_b, to_a], arecv.at[n, k - 1], a2s, a2r.at[n], device)
-    for n in range(CHUNKS):
-        cols = slice(COLS * n, COLS * (n + 1))
-        total = hid_ref[:, cols] + aown[n, colours[min(n, 1)][0], a]
-        landed(arecv.at[n], a2r.at[n])
+            start(asend.at[to_b, to_a, :, span], arecv.at[k - 1, :, span], a2s, a2r.at[n], device)
+    for n, (low, width, s) in enumerate(CHUNKS):
+        cols, span = slice(low, low + width), pl.ds(low, width)
+        total = hid_ref[:, cols] + aown[colours[s][0], a, :, cols]
+        landed(arecv.at[:, :, span], a2r.at[n])
         for k in range(15):
-            total = total + arecv[n, k].astype(f32)
+            total = total + arecv[k, :, cols].astype(f32)
         out_ref[:, cols] = total.astype(bf)
     landed(wsend.at[pl.ds(0, 7)], rs_w)
     for s in range(2):
@@ -388,18 +400,18 @@
             pltpu.VMEM((4, 4, 16, WIDE), bf),
             pltpu.VMEM((4, 4, 16, WIDE), bf),
             pltpu.VMEM((2, 256, 512), bf),
-            pltpu.VMEM((CHUNKS, 4, 4, 16, COLS), f32),
-            pltpu.VMEM((CHUNKS, 4, 4, 16, COLS), bf),
-            pltpu.VMEM((CHUNKS, 4, 4, 16, COLS), bf),
-            pltpu.VMEM((CHUNKS, 4, 4, 16, COLS), bf),
-            pltpu.VMEM((CHUNKS, 3, 4, 16, COLS), bf),
-            pltpu.VMEM((CHUNKS, 4, 16, COLS), f32),
-            pltpu.VMEM((CHUNKS, 4, 4, SEQ_DEV, COLS), f32),
-            pltpu.VMEM((CHUNKS, 4, 4, SEQ_DEV, COLS), bf),
-            pltpu.VMEM((CHUNKS, 15, SEQ_DEV, COLS), bf),
+            pltpu.VMEM((4, 4, 16, D), f32),
+            pltpu.VMEM((4, 4, 16, D), bf),
+            pltpu.VMEM((4, 4, 16, D), bf),
+            pltpu.VMEM((4, 4, 16, D), bf),
+            pltpu.VMEM((3, 4, 16, D), bf),
+            pltpu.VMEM((4, 16, D), f32),
+            pltpu.VMEM((4, 4, SEQ_DEV, D), f32),
+            pltpu.VMEM((4, 4, SEQ_DEV, D), bf),
+            pltpu.VMEM((15, SEQ_DEV, D), bf),
             dma((9,)), dma, dma((5,)), dma, dma, dma((4,)),
             dma((2,)), dma, dma, dma((2,)), dma((2, 4)), dma((2,)), dma((2, 4)), dma, dma,
-            dma, dma((CHUNKS,)), dma, dma((CHUNKS,)), dma, dma((CHUNKS,)),
+            dma, dma((4,)), dma, dma((4,)), dma, dma((4,)),
         ],
         compiler_params=pltpu.CompilerParams(
             collective_id=0, has_side_effects=True, vmem_limit_bytes=VMEM_LIMIT

time: 43.3 us -> 42.4 us (0.979)
  Pallas kernels: 42.5 us -> 41.7 us
    pallas_call x1, Pallas kernels: 41.8 us -> 41 us  [per_device(): pl.pallas_call(layer_kernel, out_shape=tuple((pltpu.VMEM(shape.shape, bf)...]
where the time goes in v5:
time: 42.4 us; the launch traced here: 42.3 us
  Pallas kernels  41.7 us (98%)
  between operations  0.65 us (2%)
    pallas_call x1, Pallas kernels, per_device(): pl.pallas_call(layer_kernel, out_shape=tuple((pltpu.VMEM(shape.shape, bf)...  41 us

profile of v5, /device:TPU:0, one launch (start us, length us, event | category | flops | bytes accessed | tf_op | source)
XLA Modules:
  0.0 42.3 jit_solution(3581269322904292548)
XLA Ops:
  0.6 41.0 %shard_map.220 = (bf16[4,2048]{1,0:T(4,128)(2,1)S(1)}, bf16[4,256]{1,0:T(4,128)(2,1)S(1)}, bf16[4,256]{1,0:T(4,128)(2,1)S(1)}) custom-call(s32[4]{0:T(128)} %len_hbm.1, f32[8]{0:T(128)} %lam_hbm.1, s32[2,4]{1,0:T(2,128)} %bitcast.23, f32[2,4]{1,0:T(2,128)} %bitcast.24, bf16[4,2048]{1,0:T(4,128)(2,1)} %tok_hbm.1, f32[1,2048]{1,0:T(1,128)} %bitcast.20, ...), custom_call_target="tpu_custom_call" | custom-call | tf_op jit(solution)/shard_map/pallas_call | solution.py:366
  41.7 0.6 %shard_map.221 = (bf16[4,2048]{1,0:T(4,128)(2,1)}, bf16[4,256]{1,0:T(4,128)(2,1)}, bf16[4,256]{1,0:T(4,128)(2,1)}) custom-call(bf16[4,2048]{1,0:T(4,128)(2,1)S(1)} %get-tuple-element.6.out_in, bf16[4,256]{1,0:T(4,128)(2,1)S(1)} %get-tuple-element.7.newk_in, bf16[4,256]{1,0:T(4,128)(2,1)S(1)} %get-tuple-element.8.newv_in), custom_call_target="tpu_custom_call" | custom-call | tf_op jit(solution)/shard_map/pallas_call | solution.py:425

commit v6 on v5

--- a/solution.py
+++ b/solution.py
@@ -89,8 +89,8 @@
         (hgain_hbm, hgain_ref), (bgate_hbm, bgate_ref),
     )
     small_in = [fetch(src, dst, isem.at[k]) for k, (src, dst) in enumerate(small)]
-    quarter = [pl.ds(256 * n, 256) for n in range(4)]
-    proj_in = [fetch(qw_hbm.at[:, part], qw.at[:, part], qsem.at[k], 1) for k, part in enumerate(quarter)]
+    quarter = [pl.ds(512 * n, 512) for n in range(4)]
+    proj_in = [fetch(qw_hbm.at[part], qw.at[part], qsem.at[k], 1) for k, part in enumerate(quarter)]
     fetch(kw_hbm, kvw.at[:, pl.ds(0, 256)], qsem.at[4], 1)
     fetch(vw_hbm, kvw.at[:, pl.ds(256, 256)], qsem.at[4], 1)
     barrier = pltpu.get_barrier_semaphore()
@@ -119,18 +119,19 @@
         start(wsend.at[to], wrecv.at[row_block], rs_w, rr_w, device)
     wrecv[row_block] = wsend[row_block]
     normed = rms_norm(tok_ref[...].astype(f32), again_ref[...], 1e-06).astype(bf)
+    query = jnp.zeros((SEQ_DEV, HEADS * HEAD_DIM), f32)
     for n in range(4):
         proj_in[n].wait()
-        cols = slice(256 * n, 256 * (n + 1))
         if n == 0:
             fetch(keys_hbm, keys, ksem, 1)
         if n == 2:
             fetch(values_hbm, values, vsem, 1)
-        qf[:, cols] = jnp.dot(normed, qw[:, cols], preferred_element_type=f32).astype(bf).astype(f32)
+        part = slice(512 * n, 512 * (n + 1))
+        query = query + jnp.dot(normed[:, part], qw[part], preferred_element_type=f32)
+    qf[:, : HEADS * HEAD_DIM] = query.astype(bf).astype(f32)
     landed(kvw, qsem.at[4])
-    out_in = [
-        fetch(ow_hbm.at[:, pl.ds(512 * n, 512)], ow.at[:, pl.ds(512 * n, 512)], osem.at[n]) for n in range(4)
-    ]
+    rows256 = [pl.ds(256 * n, 256) for n in range(4)]
+    out_in = [fetch(ow_hbm.at[part], ow.at[part], osem.at[n], 1) for n, part in enumerate(rows256)]
     new = jnp.dot(normed, kvw[...], preferred_element_type=f32).astype(bf)
     newk_ref[...] = new[:, :256]
     newv_ref[...] = new[:, 256:]
@@ -166,9 +167,9 @@
         sc[s] = lax.dot_general(both, keys[s], NT, preferred_element_type=f32) * scale
     for n in range(3):
         cols = pl.ds(128 * n, 128)
-        fetch(wg_hbm.at[:, cols], wgu.at[n, :, pl.ds(0, 128)], wsem.at[0])
-        fetch(wu_hbm.at[:, cols], wgu.at[n, :, pl.ds(128, 128)], wsem.at[0])
-    fetch(wd_hbm, wdx.at[pl.ds(0, HID)], wsem.at[1])
+        fetch(wg_hbm.at[:, cols], wgu.at[n, :, pl.ds(0, 128)], wsem.at[0], 1)
+        fetch(wu_hbm.at[:, cols], wgu.at[n, :, pl.ds(128, 128)], wsem.at[0], 1)
+    fetch(wd_hbm, wdx.at[pl.ds(0, HID)], wsem.at[1], 1)
     landed(values, vsem)
     for s in range(SEQ_DEV):
         q = qs[s]
@@ -188,11 +189,13 @@
         for h in range(HEADS):
             hf[s : s + 1, HEAD_DIM * h : HEAD_DIM * (h + 1)] = mixed[h : h + 1]
     heads = hf[...].astype(bf)
+    state = tok_ref[...].astype(f32)
     for n in range(4):
         out_in[n].wait()
-        cols = slice(512 * n, 512 * (n + 1))
-        hid_ref[:, cols] = tok_ref[:, cols].astype(f32) + jnp.dot(heads, ow[:, cols], preferred_element_type=f32)
-    ffn_in = rms_norm(hid_ref[...], fgain_ref[...], 1e-06).astype(bf)
+        part = slice(256 * n, 256 * (n + 1))
+        state = state + jnp.dot(heads[:, part], ow[part], preferred_element_type=f32)
+    hid_ref[...] = state
+    ffn_in = rms_norm(state, fgain_ref[...], 1e-06).astype(bf)
     gate_row = bgate_ref[...].astype(f32)
     terms = jnp.zeros((SEQ_DEV, 128), f32)
     for k in range(16):
@@ -280,9 +283,7 @@
         low, width, s = CHUNKS[n]
         cols, span = slice(low, low + width), pl.ds(low, width)
         landed(drecv.at[:, :, :, span], d2r.at[n])
-        total = acc[:, :, :, cols] + drecv[:, :, :, cols].astype(f32)
-        acc[:, :, :, cols] = total
-        csend[:, :, :, cols] = total.astype(bf)
+        csend[:, :, :, cols] = (acc[:, :, :, cols] + drecv[:, :, :, cols].astype(f32)).astype(bf)
         c, sc_ = colours[s][2:]
         for d in (2, 1, 3):
             to, device = ring(c, sc_, d)
@@ -310,7 +311,10 @@
         cols, span = slice(low, low + width), pl.ds(low, width)
         b, sb, c, _ = colours[s]
         landed(crecv.at[:, :, :, span], c2r.at[n])
-        total = acc[c, :, :, cols] if s == 0 else acc[:, c, :, cols]
+        if s == 0:
+            total = acc[c, :, :, cols] + drecv[c, :, :, cols].astype(f32)
+        else:
+            total = acc[:, c, :, cols] + drecv[:, c, :, cols].astype(f32)
         for d in range(3):
             total = total + crecv[d, :, :, cols].astype(f32)
         bsum[:, :, cols] = total

time: 42.4 us -> 42.3 us (level)
  no operation moved by 1% of the time
where the time goes in v6:
time: 42.3 us; the launch traced here: 42 us
  Pallas kernels  41.4 us (98%)
  between operations  0.65 us (2%)
    pallas_call x1, Pallas kernels, per_device(): pl.pallas_call(layer_kernel, out_shape=tuple((pltpu.VMEM(shape.shape, bf)...  40.7 us

profile of v6, /device:TPU:0, one launch (start us, length us, event | category | flops | bytes accessed | tf_op | source)
XLA Modules:
  0.0 42.0 jit_solution(15891981119984364549)
XLA Ops:
  0.6 40.7 %shard_map.220 = (bf16[4,2048]{1,0:T(4,128)(2,1)S(1)}, bf16[4,256]{1,0:T(4,128)(2,1)S(1)}, bf16[4,256]{1,0:T(4,128)(2,1)S(1)}) custom-call(s32[4]{0:T(128)} %len_hbm.1, f32[8]{0:T(128)} %lam_hbm.1, s32[2,4]{1,0:T(2,128)} %bitcast.23, f32[2,4]{1,0:T(2,128)} %bitcast.24, bf16[4,2048]{1,0:T(4,128)(2,1)} %tok_hbm.1, f32[1,2048]{1,0:T(1,128)} %bitcast.20, ...), custom_call_target="tpu_custom_call" | custom-call | tf_op jit(solution)/shard_map/pallas_call | solution.py:370
  41.4 0.6 %shard_map.221 = (bf16[4,2048]{1,0:T(4,128)(2,1)}, bf16[4,256]{1,0:T(4,128)(2,1)}, bf16[4,256]{1,0:T(4,128)(2,1)}) custom-call(bf16[4,2048]{1,0:T(4,128)(2,1)S(1)} %get-tuple-element.6.out_in, bf16[4,256]{1,0:T(4,128)(2,1)S(1)} %get-tuple-element.7.newk_in, bf16[4,256]{1,0:T(4,128)(2,1)S(1)} %get-tuple-element.8.newv_in), custom_call_target="tpu_custom_call" | custom-call | tf_op jit(solution)/shard_map/pallas_call | solution.py:429

commit v7 on v6

--- a/solution.py
+++ b/solution.py
@@ -240,7 +240,7 @@
             place = place_of(s, c, row)
             xown[(*place, slice(None), lanes[s])] = pack[:, lanes[s]].astype(bf)
             at = (*place, slice(None), spans[s])
-            for dc in (1, 3, 2):
+            for dc in (2, 1, 3):
                 start(xown.at[at], xown.at[at], cs_s.at[s], cs_r.at[s, db], ring(c, sc_, dc)[1])
             across(s, place)
     for db in order:

time: 42.3 us -> 42.2 us (level)
  no operation moved by 1% of the time
where the time goes in v7:
time: 42.2 us; the launch traced here: 42 us
  Pallas kernels  41.4 us (98%)
  between operations  0.65 us (2%)
    pallas_call x1, Pallas kernels, per_device(): pl.pallas_call(layer_kernel, out_shape=tuple((pltpu.VMEM(shape.shape, bf)...  40.8 us

profile of v7, /device:TPU:0, one launch (start us, length us, event | category | flops | bytes accessed | tf_op | source)
XLA Modules:
  0.0 42.0 jit_solution(8014605516758615456)
XLA Ops:
  0.6 40.8 %shard_map.220 = (bf16[4,2048]{1,0:T(4,128)(2,1)S(1)}, bf16[4,256]{1,0:T(4,128)(2,1)S(1)}, bf16[4,256]{1,0:T(4,128)(2,1)S(1)}) custom-call(s32[4]{0:T(128)} %len_hbm.1, f32[8]{0:T(128)} %lam_hbm.1, s32[2,4]{1,0:T(2,128)} %bitcast.23, f32[2,4]{1,0:T(2,128)} %bitcast.24, bf16[4,2048]{1,0:T(4,128)(2,1)} %tok_hbm.1, f32[1,2048]{1,0:T(1,128)} %bitcast.20, ...), custom_call_target="tpu_custom_call" | custom-call | tf_op jit(solution)/shard_map/pallas_call | solution.py:370
  41.4 0.6 %shard_map.221 = (bf16[4,2048]{1,0:T(4,128)(2,1)}, bf16[4,256]{1,0:T(4,128)(2,1)}, bf16[4,256]{1,0:T(4,128)(2,1)}) custom-call(bf16[4,2048]{1,0:T(4,128)(2,1)S(1)} %get-tuple-element.6.out_in, bf16[4,256]{1,0:T(4,128)(2,1)S(1)} %get-tuple-element.7.newk_in, bf16[4,256]{1,0:T(4,128)(2,1)S(1)} %get-tuple-element.8.newv_in), custom_call_target="tpu_custom_call" | custom-call | tf_op jit(solution)/shard_map/pallas_call | solution.py:429

commit v8 on v7

--- a/solution.py
+++ b/solution.py
@@ -113,6 +113,7 @@
             wsend[r, PART * k : PART * (k + 1)] = tiles[k, PART * r : PART * (r + 1)]
         wsend[7, PART * k : PART * k + 16] = tiles[k, 336:352]
         wsend[7, PART * k + 16 : PART * (k + 1)] = jnp.zeros((32, 256), bf)
+    fetch(keys_hbm, keys, ksem, 1)
     pl.semaphore_wait(barrier, 38)
     for d in range(1, 8):
         to, device = group(d)
@@ -122,8 +123,6 @@
     query = jnp.zeros((SEQ_DEV, HEADS * HEAD_DIM), f32)
     for n in range(4):
         proj_in[n].wait()
-        if n == 0:
-            fetch(keys_hbm, keys, ksem, 1)
         if n == 2:
             fetch(values_hbm, values, vsem, 1)
         part = slice(512 * n, 512 * (n + 1))

time: 42.2 us -> 42.2 us (level)
  no operation moved by 1% of the time
where the time goes in v8:
time: 42.2 us; the launch traced here: 42 us
  Pallas kernels  41.3 us (98%)
  between operations  0.65 us (2%)
    pallas_call x1, Pallas kernels, per_device(): pl.pallas_call(layer_kernel, out_shape=tuple((pltpu.VMEM(shape.shape, bf)...  40.7 us

profile of v8, /device:TPU:0, one launch (start us, length us, event | category | flops | bytes accessed | tf_op | source)
XLA Modules:
  0.0 42.0 jit_solution(5435765917493690483)
XLA Ops:
  0.6 40.7 %shard_map.220 = (bf16[4,2048]{1,0:T(4,128)(2,1)S(1)}, bf16[4,256]{1,0:T(4,128)(2,1)S(1)}, bf16[4,256]{1,0:T(4,128)(2,1)S(1)}) custom-call(s32[4]{0:T(128)} %len_hbm.1, f32[8]{0:T(128)} %lam_hbm.1, s32[2,4]{1,0:T(2,128)} %bitcast.23, f32[2,4]{1,0:T(2,128)} %bitcast.24, bf16[4,2048]{1,0:T(4,128)(2,1)} %tok_hbm.1, f32[1,2048]{1,0:T(1,128)} %bitcast.20, ...), custom_call_target="tpu_custom_call" | custom-call | tf_op jit(solution)/shard_map/pallas_call | solution.py:369
  41.4 0.6 %shard_map.221 = (bf16[4,2048]{1,0:T(4,128)(2,1)}, bf16[4,256]{1,0:T(4,128)(2,1)}, bf16[4,256]{1,0:T(4,128)(2,1)}) custom-call(bf16[4,2048]{1,0:T(4,128)(2,1)S(1)} %get-tuple-element.6.out_in, bf16[4,256]{1,0:T(4,128)(2,1)S(1)} %get-tuple-element.7.newk_in, bf16[4,256]{1,0:T(4,128)(2,1)S(1)} %get-tuple-element.8.newv_in), custom_call_target="tpu_custom_call" | custom-call | tf_op jit(solution)/shard_map/pallas_call | solution.py:428
